TPU v7x, 32 devices: a whole 2x2x4 slice. The times are simulated.
32 devices in a mesh: sp: 8 (over z, x), tp: 4 (over y, core).
Axes of the slice: x: 2, y: 2, z: 4, core: 2. Of those that a mesh axis runs over, the one named last changes fastest.
Arguments:
- cotangent: bfloat16 [2048, 2048], P('sp'), may hold values from -6 to 6
- route_ids: int32 [2048, 2], P('sp'), may hold values from 0 to 7, all different within a row; in each aligned block of 256 rows (0 to 255, 256 to 511, ...) at most 128 rows name the same one
- route_weights: float32 [2048, 2], P('sp'), may hold values from 0.2 to 1
- expert_inputs: bfloat16 [8, 1024, 2048], P('sp'), may hold values from -6 to 6
- gate_weight: bfloat16 [8, 2048, 1024], P('sp', None, 'tp'), may hold values from -0.125 to 0.125
- up_weight: bfloat16 [8, 2048, 1024], P('sp', None, 'tp'), may hold values from -0.125 to 0.125
- down_weight: bfloat16 [8, 1024, 2048], P('sp', 'tp'), may hold values from -0.1875 to 0.1875
- out_weight: bfloat16 [2048, 512], P(None, 'tp'), may hold values from -0.25 to 0.25
- gate_in: bfloat16 [2048, 512], P('sp', 'tp'), may hold values from -6 to 6
- conv_sum: bfloat16 [2048, 512], P('sp', 'tp'), may hold values from -6 to 6
- conv_c: bfloat16 [2048, 512], P('sp', 'tp'), may hold values from -6 to 6
- conv_v: bfloat16 [2048, 512], P('sp', 'tp'), may hold values from -6 to 6
- conv_taps: float32 [3, 512], P(None, 'tp'), may hold values from -3 to 3
Outputs:
- grad_input: bfloat16 [2048, 2048], P('sp', 'tp')
- grad_gate: bfloat16 [8, 2048, 1024], P('sp', None, 'tp')
- grad_up: bfloat16 [8, 2048, 1024], P('sp', None, 'tp')
- grad_down: bfloat16 [8, 1024, 2048], P('sp', 'tp')
- grad_out_weight: float32 [2048, 512], P('sp', 'tp')
- grad_gate_in: bfloat16 [2048, 512], P('sp', 'tp')
- grad_conv_c: bfloat16 [2048, 512], P('sp', 'tp')
- grad_conv_v: bfloat16 [2048, 512], P('sp', 'tp')
Inputs may be any that keep to these rules, and one draw needn't show every extreme that they name: `route_ids`: the 2 experts of a token differ. Among the 256 tokens of one index of sp no expert is named more than 128 times, and in every draw some expert is named exactly 128 times by the tokens of some index of sp.
All inputs are finite; a program needn't handle non-finite values.
Results may differ from a plain program's by a relative error of at most 0.012.
Values may be sent and summed in bfloat16 or wider, within the bound.
No kernel may reach another device: no remote copies, remote signals or barrier semaphores. Data moves between devices by JAX's collectives and lax.ppermute only.
A program may use at most 128 MiB of HBM per device.

v0:
```python
import functools

import jax
import jax.numpy as jnp
from jax import lax
from jax.experimental import pallas as pl
from jax.experimental.pallas import tpu as pltpu
from jax.sharding import PartitionSpec as P


F32 = jnp.float32
BF16 = jnp.bfloat16


def dot(a, b, contract):
    return lax.dot_general(a, b, (contract, ((), ())), preferred_element_type=F32)


def swap(value, axis, distance):
    route = [(i, i ^ distance) for i in range(lax.axis_size(axis))]
    return lax.ppermute(value, axis, route)


def position(direct):
    me = lax.axis_index("sp")
    return (me if direct else 0), me, lax.axis_index("tp")


def routing(ids, weights, experts, capacity, order):
    tokens = ids.shape[1]
    slots = experts * capacity
    labels = ids[...] ^ order
    expert = lax.broadcasted_iota(jnp.int32, (experts, tokens), 0)
    hit = jnp.zeros((experts, tokens), F32)
    factor = jnp.zeros((experts, tokens), F32)
    for k in range(labels.shape[0]):
        same = expert == labels[k : k + 1]
        hit = hit + same.astype(F32)
        factor = factor + jnp.where(same, weights[k : k + 1], 0.0)
    earlier = (
        lax.broadcasted_iota(jnp.int32, (tokens, tokens), 0)
        < lax.broadcasted_iota(jnp.int32, (tokens, tokens), 1)
    ).astype(F32)
    before = dot(hit.astype(BF16), earlier.astype(BF16), ((1,), (0,))).astype(jnp.int32)
    rank = jnp.where(hit > 0, before, -1)
    row = lax.broadcasted_iota(jnp.int32, (experts, capacity, tokens), 1)
    chosen = (rank[:, None, :] == row).astype(F32)
    scale = jnp.sum(chosen * factor[:, None, :], axis=2, keepdims=True).reshape(slots, 1)
    return chosen.reshape(slots, tokens), scale


def lane_columns_of(ref, lane, cols):
    return ref.at[:, pl.ds(pl.multiple_of(lane * cols, cols), cols)]


def in_hbm(*arrays):
    return [pltpu.with_memory_space_constraint(a, pltpu.HBM) for a in arrays]


def lane_columns(ref, lane, cols):
    return ref[:, pl.ds(pl.multiple_of(lane * cols, cols), cols)]


def dispatch_kernel(experts, direct, ids_in, weights_in, cot_in, *refs):
    blocks, (ids, weights, cot, sems) = refs[:-4], refs[-4:]
    order, _, lane = position(direct)
    capacity = blocks[0].shape[0] if direct else blocks[0].shape[0] // experts
    cols = cot.shape[1]
    copies = [
        pltpu.make_async_copy(ids_in, ids, sems.at[0]),
        pltpu.make_async_copy(weights_in, weights, sems.at[1]),
        pltpu.make_async_copy(lane_columns_of(cot_in, lane, cols), cot, sems.at[2]),
    ]
    for copy in copies:
        copy.start()
    copies[0].wait()
    copies[1].wait()
    chosen, scale = routing(ids, weights, experts, capacity, order)
    copies[2].wait()
    rows = dot(chosen.astype(BF16), cot[...], ((1,), (0,))) * scale
    if direct:
        for k in range(1, experts):
            blocks[k - 1][...] = rows[k * capacity : (k + 1) * capacity].astype(BF16)
    else:
        blocks[0][...] = rows.astype(BF16)


def local_kernel(lanes, experts, capacity, direct, ids_in, weights_in, cot_in, *refs):
    select, own_cot, *pieces = refs[:-4]
    ids, weights, cot, sems = refs[-4:]
    order, _, lane = position(direct)
    cols = cot.shape[1] // lanes
    copies = [
        pltpu.make_async_copy(ids_in, ids, sems.at[0]),
        pltpu.make_async_copy(weights_in, weights, sems.at[1]),
        pltpu.make_async_copy(cot_in, cot, sems.at[2]),
    ]
    for copy in copies:
        copy.start()
    for copy in copies:
        copy.wait()
    chosen, scale = routing(ids, weights, experts, capacity, order)
    select[...] = chosen.T.astype(BF16)
    own_cot[...] = lane_columns(cot, lane, cols)
    if direct:
        first = chosen[:capacity].astype(BF16)
        for j in range(lanes):
            rows = dot(first, lane_columns(cot, lane ^ j, cols), ((1,), (0,)))
            pieces[j][...] = (rows * scale[:capacity]).astype(BF16)


def pre_kernel(capacity, info, x, w_gate, w_up, hidden, slope, swish):
    gate = dot(x[...], w_gate[...], ((1,), (0,)))
    up = dot(x[...], w_up[...], ((1,), (0,)))
    sig = jax.nn.sigmoid(gate)
    silu = gate * sig
    deriv = up * sig * (1.0 + gate * (1.0 - sig))
    keep = (silu * up).astype(BF16)
    pack = x.shape[0] // capacity
    for i in range(pack):
        part = slice(i * capacity, (i + 1) * capacity)
        place = ((info[0] ^ i) & (pack - 1)) * capacity
        spot = pl.ds(pl.multiple_of(place, capacity), capacity)
        hidden[spot, :] = keep[part]
        slope[spot, :] = deriv[part]
        swish[spot, :] = silu[part]


def mid_kernel(lanes, first, slope, swish, w_gate, w_up, w_down, *refs):
    pieces, (d_gate, d_up), outs = refs[:lanes], refs[lanes : lanes + 2], refs[lanes + 2 :]
    rows, cols = pieces[0].shape
    lane = lax.axis_index("tp")
    part = slice(first, first + rows)
    total = None
    for j in range(lanes):
        term = dot(pieces[j][...], lane_columns(w_down, lane ^ j, cols), ((1,), (1,)))
        total = term if total is None else total + term
    gate = (total * slope[part, :]).astype(BF16)
    up = (total * swish[part, :]).astype(BF16)
    d_gate[...] = gate
    d_up[...] = up
    for j in range(lanes):
        spot = pl.ds(pl.multiple_of((lane ^ j) * cols, cols), cols)
        out = dot(gate, w_gate[spot, :], ((1,), (1,))) + dot(up, w_up[spot, :], ((1,), (1,)))
        outs[j][...] = out.astype(BF16)


def down_kernel(lanes, count, hidden, *refs):
    pieces, out = refs[:-1], refs[-1]
    cols = out.shape[1] // lanes
    lane = lax.axis_index("tp")
    for j in range(lanes):
        total = None
        start = 0
        for g in range(count):
            piece = pieces[g * lanes + j]
            size = piece.shape[0]
            term = dot(hidden[start : start + size], piece[...], ((0,), (0,)))
            total = term if total is None else total + term
            start += size
        spot = pl.ds(pl.multiple_of((lane ^ j) * cols, cols), cols)
        out[:, spot] = total.astype(BF16)


def gate_up_kernel(capacity, count, direct, x, *refs):
    grads, (out_gate, out_up) = refs[: 2 * count], refs[2 * count :]
    order, _, _ = position(direct)
    gates, ups = None, None
    k = 0
    for g in range(count):
        gate, up = grads[2 * g], grads[2 * g + 1]
        for i in range(gate.shape[0] // capacity):
            spot = pl.ds(pl.multiple_of((order ^ k) * capacity, capacity), capacity)
            part = slice(i * capacity, (i + 1) * capacity)
            rows = x[spot, :]
            one = dot(rows, gate[part], ((0,), (0,)))
            two = dot(rows, up[part], ((0,), (0,)))
            gates = one if gates is None else gates + one
            ups = two if ups is None else ups + two
            k += 1
    out_gate[...] = gates.astype(BF16)
    out_up[...] = ups.astype(BF16)


def combine_kernel(select, cot, *refs):
    blocks, (out, kept) = refs[:-2], refs[-2:]
    total = cot[...].astype(F32)
    start = 0
    for block in blocks:
        size = block.shape[0]
        total = total + dot(select[:, start : start + size], block[...], ((1,), (0,)))
        start += size
    out[...] = total.astype(BF16)
    kept[...] = total.astype(BF16)


def mixer_kernel(lanes, direct, gate_in, conv_sum, w_out, *refs):
    pieces = refs[:lanes]
    d_gate_in, d_sum = refs[lanes : lanes + 2]
    own, outs, scratch = refs[lanes + 2], refs[lanes + 3 : -1], refs[-1]
    cols = pieces[0].shape[1]
    order, me, lane = position(direct)
    gate = gate_in[...].astype(F32)
    conv = conv_sum[...].astype(F32)
    mixed = (gate * conv).astype(BF16)
    total = None
    for j in range(lanes):
        spot = pl.ds(pl.multiple_of((lane ^ j) * cols, cols), cols)
        piece = pieces[j][...]
        term = dot(piece, w_out[spot, :], ((1,), (0,)))
        total = term if total is None else total + term
        scratch[spot, :] = dot(piece, mixed, ((0,), (0,)))
    d_gate_in[...] = (total * conv).astype(BF16)
    d_sum[...] = total * gate
    size = own.shape[0]
    if direct:
        for k in range(scratch.shape[0] // size):
            part = scratch[pl.ds(pl.multiple_of((order ^ k) * size, size), size), :]
            if k == 0:
                own[...] = part
            else:
                outs[k - 1][...] = part.astype(BF16)
    else:
        own[...] = scratch[pl.ds(pl.multiple_of(me * size, size), size), :]
        outs[0][...] = scratch[...].astype(BF16)


def flat_call(kernel, ins, outs, flops, limit, scratch=(), space=pltpu.VMEM):
    return pl.pallas_call(
        kernel,
        in_specs=[pl.BlockSpec(memory_space=space)] * len(ins),
        out_specs=[pl.BlockSpec(memory_space=pltpu.VMEM)] * len(outs),
        out_shape=outs,
        scratch_shapes=list(scratch),
        compiler_params=pltpu.CompilerParams(vmem_limit_bytes=limit << 20),
        cost_estimate=pl.CostEstimate(
            flops=flops,
            transcendentals=0,
            bytes_accessed=sum(a.size * a.dtype.itemsize for a in [*ins, *outs]),
        ),
    )(*ins)


def struct(shape, dtype):
    return jax.ShapeDtypeStruct(shape, dtype)


def gather_lanes(own, lanes):
    distance = lanes // 2
    have = {0: own}
    while distance >= 1:
        for j in list(have):
            k = j ^ distance
            have[k] = swap(have[j], "tp", distance)
        distance //= 2
    return [have[j] for j in range(lanes)]


def sum_lanes(parts, lanes):
    have = {j: parts[j].astype(F32) for j in range(lanes)}
    distance = 1
    while distance < lanes:
        sent = {j: swap(have[j].astype(BF16), "tp", distance) for j in have if j & distance}
        have = {
            j: have[j] + sent[j ^ distance].astype(F32) for j in have if not j & distance
        }
        distance *= 2
    return have[0].astype(BF16)


def body(
    cotangent,
    route_ids,
    route_weights,
    expert_inputs,
    gate_weight,
    up_weight,
    down_weight,
    out_weight,
    gate_in,
    conv_sum,
    conv_c,
    conv_v,
    conv_taps,
):
    groups = lax.axis_size("sp")
    lanes = lax.axis_size("tp")
    capacity = expert_inputs.shape[1] // groups
    tokens, model_width = cotangent.shape
    cols = model_width // lanes
    units = gate_weight.shape[2]
    slots = groups * capacity
    channels = gate_in.shape[1]
    part_rows = model_width // groups
    if gate_weight.shape[0] != 1 or lanes & (lanes - 1):
        raise ValueError("unsupported mesh")
    direct = groups == 8
    me = lax.axis_index("sp")
    order = me if direct else jnp.zeros_like(me)
    x = expert_inputs[0]
    w_gate, w_up, w_down = gate_weight[0], up_weight[0], down_weight[0]
    members = [[0], [1, 2, 3], [4, 5], [6, 7]] if direct else [list(range(groups))]
    ids, factors = route_ids.T, route_weights.T
    block = struct((capacity, cols), BF16)

    blocks = flat_call(
        functools.partial(dispatch_kernel, groups, direct),
        in_hbm(ids, factors, cotangent),
        [block] * (groups - 1) if direct else [struct((slots, cols), BF16)],
        2 * slots * tokens * cols,
        14,
        scratch=[
            pltpu.VMEM(ids.shape, jnp.int32),
            pltpu.VMEM(ids.shape, F32),
            pltpu.VMEM((tokens, cols), BF16),
            pltpu.SemaphoreType.DMA((3,)),
        ],
        space=pltpu.HBM,
    )
    select, own_cot, *own_pieces = flat_call(
        functools.partial(local_kernel, lanes, groups, capacity, direct),
        in_hbm(ids, factors, cotangent),
        [struct((tokens, slots), BF16), struct((tokens, cols), BF16)]
        + ([block] * lanes if direct else []),
        2 * slots * tokens * cols,
        14,
        scratch=[
            pltpu.VMEM(ids.shape, jnp.int32),
            pltpu.VMEM(ids.shape, F32),
            pltpu.VMEM((tokens, model_width), BF16),
            pltpu.SemaphoreType.DMA((3,)),
        ],
        space=pltpu.HBM,
    )
    pack = min(groups, 4)
    span = pl.BlockSpec((pack * capacity, units), lambda k, info: (k, 0))
    weights = pl.BlockSpec((model_width, units), lambda k, info: (0, 0))
    hidden, slope, swish = pl.pallas_call(
        functools.partial(pre_kernel, capacity),
        grid_spec=pltpu.PrefetchScalarGridSpec(
            num_scalar_prefetch=1,
            grid=(groups // pack,),
            in_specs=[
                pl.BlockSpec(
                    (pack * capacity, model_width), lambda k, info: ((info[0] // pack) ^ k, 0)
                ),
                weights,
                weights,
            ],
            out_specs=[span] * 3,
        ),
        out_shape=[
            struct((slots, units), BF16),
            struct((slots, units), F32),
            struct((slots, units), F32),
        ],
        compiler_params=pltpu.CompilerParams(vmem_limit_bytes=20 << 20),
        cost_estimate=pl.CostEstimate(
            flops=4 * slots * model_width * units,
            transcendentals=slots * units,
            bytes_accessed=12 << 20,
        ),
        name="pre",
    )(order.astype(jnp.int32)[None], *in_hbm(x, w_gate, w_up))

    def arrive(ks):
        if not direct:
            value = blocks[0].reshape(groups, capacity, cols)
            value = lax.all_to_all(value, "sp", split_axis=0, concat_axis=0, tiled=True)
            return gather_lanes(value.reshape(slots, cols), lanes)
        if ks == [0]:
            return own_pieces
        got = [swap(blocks[k - 1], "sp", k) for k in ks]
        return gather_lanes(jnp.concatenate(got, axis=0), lanes)

    arrived = {}
    for g in reversed(range(len(members))):
        arrived[g] = arrive(members[g])

    grads, returned = {}, {}
    for g, ks in enumerate(members):
        rows = len(ks) * capacity
        gate, up, *parts = flat_call(
            functools.partial(mid_kernel, lanes, ks[0] * capacity),
            (slope, swish, w_gate, w_up, w_down, *arrived[g]),
            [struct((rows, units), BF16)] * 2 + [struct((rows, cols), BF16)] * lanes,
            6 * rows * model_width * units,
            14,
        )
        grads[g] = (gate, up)
        total = sum_lanes(parts, lanes)
        if not direct:
            total = total.reshape(groups, capacity, cols)
            total = lax.all_to_all(total, "sp", split_axis=0, concat_axis=0, tiled=True)
            returned[0] = total.reshape(slots, cols)
        else:
            for i, k in enumerate(ks):
                one = total[i * capacity : (i + 1) * capacity]
                returned[k] = swap(one, "sp", k) if k else one

    count = len(members)
    flat = [piece for g in range(count) for piece in arrived[g]]
    (grad_down,) = flat_call(
        functools.partial(down_kernel, lanes, count),
        (hidden, *flat),
        [struct((units, model_width), BF16)],
        2 * slots * model_width * units,
        16,
    )
    flat = [grad for g in range(count) for grad in grads[g]]
    grad_gate, grad_up = flat_call(
        functools.partial(gate_up_kernel, capacity, count, direct),
        (x, *flat),
        [struct((model_width, units), BF16)] * 2,
        4 * slots * model_width * units,
        28,
    )
    grad_input, kept = flat_call(
        combine_kernel,
        (select, own_cot, *[returned[k] for k in sorted(returned)]),
        [struct((tokens, cols), BF16)] * 2,
        2 * slots * tokens * cols,
        16,
    )
    pieces = gather_lanes(kept, lanes)
    part = struct((part_rows, channels), BF16)
    outs = [part] * (groups - 1) if direct else [struct((model_width, channels), BF16)]
    shapes = [
        struct((tokens, channels), BF16),
        struct((tokens, channels), F32),
        struct((part_rows, channels), F32),
    ] + outs
    grad_gate_in, grad_sum, own, *terms = flat_call(
        functools.partial(mixer_kernel, lanes, direct),
        (gate_in, conv_sum, out_weight, *pieces),
        shapes,
        4 * tokens * model_width * channels,
        16,
        scratch=[pltpu.VMEM((model_width, channels), F32)],
    )
    back = [(i, i - 1) for i in range(1, groups)]
    next_rows = lax.ppermute(grad_sum[:2], "sp", back)
    if direct:
        grad_out_weight = own
        for k in range(1, groups):
            term = swap(terms[k - 1], "sp", k)
            grad_out_weight = grad_out_weight + term.astype(F32)
    else:
        value = terms[0].reshape(groups, part_rows, channels)
        value = lax.all_to_all(value, "sp", split_axis=0, concat_axis=0, tiled=True)
        others = (jnp.arange(groups) != me)[:, None, None]
        grad_out_weight = own + jnp.sum(jnp.where(others, value.astype(F32), 0.0), axis=0)
    extended = jnp.concatenate([grad_sum, next_rows], axis=0)
    grad_prod = (
        conv_taps[0] * extended[2:] + conv_taps[1] * extended[1:-1] + conv_taps[2] * extended[:-2]
    )
    grad_conv_c = (grad_prod * conv_v.astype(F32)).astype(BF16)
    grad_conv_v = (grad_prod * conv_c.astype(F32)).astype(BF16)
    return (
        grad_input,
        grad_gate[None],
        grad_up[None],
        grad_down[None],
        grad_out_weight,
        grad_gate_in,
        grad_conv_c,
        grad_conv_v,
    )


def solution(mesh):
    placed = (
        P("sp", None),
        P("sp", None),
        P("sp", None),
        P("sp", None, None),
        P("sp", None, "tp"),
        P("sp", None, "tp"),
        P("sp", "tp", None),
        P(None, "tp"),
        P("sp", "tp"),
        P("sp", "tp"),
        P("sp", "tp"),
        P("sp", "tp"),
        P(None, "tp"),
    )
    return jax.shard_map(
        body,
        mesh=mesh,
        in_specs=placed,
        out_specs=(
            P("sp", "tp"),
            P("sp", None, "tp"),
            P("sp", None, "tp"),
            P("sp", "tp", None),
            P("sp", "tp"),
            P("sp", "tp"),
            P("sp", "tp"),
            P("sp", "tp"),
        ),
        check_vma=False,
    )
```

profile of v0, /device:TPU:0, one launch (start us, length us, event | category | flops | bytes accessed | tf_op | source)
XLA Modules:
  0.0 135.7 jit_solution(17265303699113752994)
XLA Ops:
  2.3 5.1 %collective-permute-start.25 = (bf16[128,512]{1,0:T(8,128)(2,1)S(1)}, bf16[128,512]{1,0:T(8,128)(2,1)S(1)}, u32[]{:S(2)}, u32[]{:S(2)}) collective-permute-start(bf16[128,512]{1,0:T(8,128)(2,1)S(1)} %get-tuple-element.87), channel_id=1, source_target_pairs={{0,24},{4,28},{8,16},{12,20},{16,8},{20,12},{24,0},{28,4},{1,25},{... | collective-permute-start | bytes 393224 | tf_op jit(solution)/shard_map/ppermute | solution.py:21
  14.8 8.1 %collective-permute-start.4 = (bf16[128,512]{1,0:T(8,128)(2,1)S(1)}, bf16[128,512]{1,0:T(8,128)(2,1)S(1)}, u32[]{:S(2)}, u32[]{:S(2)}) collective-permute-start(bf16[128,512]{1,0:T(8,128)(2,1)S(1)} %get-tuple-element.75), channel_id=1, source_target_pairs={{0,8},{4,12},{8,0},{12,4},{16,24},{20,28},{24,16},{28,20},{1,9},{5... | collective-permute-start | bytes 393224 | tf_op jit(solution)/shard_map/ppermute | solution.py:21
  22.8 3.7 %collective-permute-start.5 = (bf16[128,512]{1,0:T(8,128)(2,1)S(1)}, bf16[128,512]{1,0:T(8,128)(2,1)S(1)}, u32[]{:S(2)}, u32[]{:S(2)}) collective-permute-start(bf16[128,512]{1,0:T(8,128)(2,1)S(1)} %get-tuple-element.76), channel_id=1, source_target_pairs={{0,12},{4,8},{8,4},{12,0},{16,28},{20,24},{24,20},{28,16},{1,13},{... | collective-permute-start | bytes 393224 | tf_op jit(solution)/shard_map/ppermute | solution.py:21
  28.1 3.6 %collective-permute-done.4 = bf16[128,512]{1,0:T(8,128)(2,1)S(1)} collective-permute-done((bf16[128,512]{1,0:T(8,128)(2,1)S(1)}, bf16[128,512]{1,0:T(8,128)(2,1)S(1)}, u32[]{:S(2)}, u32[]{:S(2)}) %collective-permute-start.4) | collective-permute-done | bytes 131104 | tf_op jit(solution)/shard_map/ppermute | solution.py:21
  31.7 2.8 %collective-permute-done.5 = bf16[128,512]{1,0:T(8,128)(2,1)S(1)} collective-permute-done((bf16[128,512]{1,0:T(8,128)(2,1)S(1)}, bf16[128,512]{1,0:T(8,128)(2,1)S(1)}, u32[]{:S(2)}, u32[]{:S(2)}) %collective-permute-start.5) | collective-permute-done | bytes 131104 | tf_op jit(solution)/shard_map/ppermute | solution.py:21
  36.8 5.0 %pre.1 = (bf16[1024,256]{1,0:T(8,128)(2,1)S(1)}, f32[1024,256]{1,0:T(8,128)S(1)}, f32[1024,256]{1,0:T(8,128)S(1)}) custom-call(s32[1]{0:T(128)} %bitcast.2.info, bf16[1024,2048]{1,0:T(8,128)(2,1)} %bitcast.30, bf16[2048,256]{1,0:T(8,128)(2,1)} %bitcast.16, bf16[2048,256]{1,0:T(8,128)(2,1)} %bitcast.21), custom_call_target="tpu_custom_call" | custom-call | flops 2147483648 | bytes 12582912 | tf_op jit(solution)/shard_map/pre/pallas_call | solution.py:338
  44.2 6.0 %collective-permute-done.18.refs_2_.refs_10_ = bf16[256,512]{1,0:T(8,128)(2,1)S(1)} collective-permute-done((bf16[256,512]{1,0:T(8,128)(2,1)S(1)}, bf16[256,512]{1,0:T(8,128)(2,1)S(1)}, u32[]{:S(2)}, u32[]{:S(2)}) %collective-permute-start.18) | collective-permute-done | bytes 262176 | tf_op jit(solution)/shard_map/ppermute | solution.py:21
  57.4 2.3 %shard_map.191 = (bf16[384,256]{1,0:T(8,128)(2,1)S(1)}, bf16[384,256]{1,0:T(8,128)(2,1)S(1)}, bf16[384,512]{1,0:T(8,128)(2,1)S(1)}, bf16[384,512]{1,0:T(8,128)(2...) custom-call(f32[1024,256]{1,0:T(8,128)S(1)} %get-tuple-element.64.slope, ...), custom_call_target="tpu_custom_call" | custom-call | flops 1207959552 | bytes 8781824 | tf_op jit(solution)/shard_map/pallas_call | solution.py:229
  61.5 4.6 %collective-permute-done.32 = bf16[256,512]{1,0:T(8,128)(2,1)S(1)} collective-permute-done((bf16[256,512]{1,0:T(8,128)(2,1)S(1)}, bf16[256,512]{1,0:T(8,128)(2,1)S(1)}, u32[]{:S(2)}, u32[]{:S(2)}) %collective-permute-start.32) | collective-permute-done | bytes 262176 | tf_op jit(solution)/shard_map/ppermute | solution.py:21
  68.1 2.0 %collective-permute-start.33 = (bf16[128,512]{1,0:T(8,128)(2,1)S(1)}, bf16[128,512]{1,0:T(8,128)(2,1)S(1)}, u32[]{:S(2)}, u32[]{:S(2)}) collective-permute-start(bf16[128,512]{1,0:T(8,128)(2,1)S(1)} %get-tuple-element.122), channel_id=1, source_target_pairs={{0,24},{4,28},{8,16},{12,20},{16,8},{20,12},{24,0},{28,4},{1,25},{... | collective-permute-start | bytes 393224 | tf_op jit(solution)/shard_map/ppermute | solution.py:21
  71.8 2.8 %collective-permute-start.34 = (bf16[128,512]{1,0:T(8,128)(2,1)S(1)}, bf16[128,512]{1,0:T(8,128)(2,1)S(1)}, u32[]{:S(2)}, u32[]{:S(2)}) collective-permute-start(bf16[128,512]{1,0:T(8,128)(2,1)S(1)} %get-tuple-element.121), channel_id=1, source_target_pairs={{0,28},{4,24},{8,20},{12,16},{16,12},{20,8},{24,4},{28,0},{1,29},{... | collective-permute-start | bytes 393224 | tf_op jit(solution)/shard_map/ppermute | solution.py:21
  74.6 6.6 %collective-permute-done.11 = bf16[384,512]{1,0:T(8,128)(2,1)S(1)} collective-permute-done((bf16[384,512]{1,0:T(8,128)(2,1)S(1)}, bf16[384,512]{1,0:T(8,128)(2,1)S(1)}, u32[]{:S(2)}, u32[]{:S(2)}) %collective-permute-start.11) | collective-permute-done | bytes 393248 | tf_op jit(solution)/shard_map/ppermute | solution.py:21
  81.4 3.8 %collective-permute-start.24 = (bf16[128,512]{1,0:T(8,128)(2,1)S(1)}, bf16[128,512]{1,0:T(8,128)(2,1)S(1)}, u32[]{:S(2)}, u32[]{:S(2)}) collective-permute-start(bf16[128,512]{1,0:T(8,128)(2,1)S(1)} %get-tuple-element.123), channel_id=1, source_target_pairs={{0,20},{4,16},{8,28},{12,24},{16,4},{20,0},{24,12},{28,8},{1,21},{... | collective-permute-start | bytes 393224 | tf_op jit(solution)/shard_map/ppermute | solution.py:21
  85.9 2.8 %collective-permute-start.14 = (bf16[128,512]{1,0:T(8,128)(2,1)S(1)}, bf16[128,512]{1,0:T(8,128)(2,1)S(1)}, u32[]{:S(2)}, u32[]{:S(2)}) collective-permute-start(bf16[128,512]{1,0:T(8,128)(2,1)S(1)} %get-tuple-element.118), channel_id=1, source_target_pairs={{0,12},{4,8},{8,4},{12,0},{16,28},{20,24},{24,20},{28,16},{1,13},{... | collective-permute-start | bytes 393224 | tf_op jit(solution)/shard_map/ppermute | solution.py:21
  88.8 3.1 %collective-permute-done.23.refs_4_ = bf16[128,512]{1,0:T(8,128)(2,1)S(1)} collective-permute-done((bf16[128,512]{1,0:T(8,128)(2,1)S(1)}, bf16[128,512]{1,0:T(8,128)(2,1)S(1)}, u32[]{:S(2)}, u32[]{:S(2)}) %collective-permute-start.23) | collective-permute-done | bytes 131104 | tf_op jit(solution)/shard_map/ppermute | solution.py:21
  91.9 2.6 %collective-permute-done.24.refs_5_ = bf16[128,512]{1,0:T(8,128)(2,1)S(1)} collective-permute-done((bf16[128,512]{1,0:T(8,128)(2,1)S(1)}, bf16[128,512]{1,0:T(8,128)(2,1)S(1)}, u32[]{:S(2)}, u32[]{:S(2)}) %collective-permute-start.24) | collective-permute-done | bytes 131104 | tf_op jit(solution)/shard_map/ppermute | solution.py:21
  95.2 2.5 %collective-permute-done.14.refs_3_ = bf16[128,512]{1,0:T(8,128)(2,1)S(1)} collective-permute-done((bf16[128,512]{1,0:T(8,128)(2,1)S(1)}, bf16[128,512]{1,0:T(8,128)(2,1)S(1)}, u32[]{:S(2)}, u32[]{:S(2)}) %collective-permute-start.14) | collective-permute-done | bytes 131104 | tf_op jit(solution)/shard_map/ppermute | solution.py:21
  99.6 5.9 %collective-permute-done.36.refs_2_ = bf16[256,512]{1,0:T(8,128)(2,1)S(1)} collective-permute-done((bf16[256,512]{1,0:T(8,128)(2,1)S(1)}, bf16[256,512]{1,0:T(8,128)(2,1)S(1)}, u32[]{:S(2)}, u32[]{:S(2)}) %collective-permute-start.36) | collective-permute-done | bytes 262176 | tf_op jit(solution)/shard_map/ppermute | solution.py:21
  105.5 2.5 %shard_map.196 = bf16[256,2048]{1,0:T(8,128)(2,1)} custom-call(bf16[1024,256]{1,0:T(8,128)(2,1)S(1)} %get-tuple-element.104.hidden, bf16[128,512]{1,0:T(8,128)(2,1)S(1)} %get-tuple-element.66.refs_0_, bf16[128,512]{1,0:T(8,128)(2,1)S(1)} %get-tuple-element.67.refs_1_, bf16[128,512]{1,0:T(8,128)(2,1)S(1)} %get-tuple-element.68.refs_2_, ...), custom_call_target="tpu_custom_call" | custom-call | flops 1073741824 | bytes 5767168 | tf_op jit(solution)/shard_map/pallas_call | solution.py:229
  108.0 5.9 %shard_map.195 = (bf16[2048,256]{1,0:T(8,128)(2,1)}, bf16[2048,256]{1,0:T(8,128)(2,1)}) custom-call(bf16[1024,2048]{1,0:T(8,128)(2,1)S(1)} %bitcast.31, bf16[128,256]{1,0:T(8,128)(2,1)S(1)} %get-tuple-element.94.refs_0_, bf16[128,256]{1,0:T(8,128)(2,1)S(1)} %get-tuple-element.95.refs_1_, bf16[384,256]{1,0:T(8,128)(2,1)S(1)} %get-tuple-element.96.refs_2_, ...), custom_call_target="tpu_custom_call" | custom-call | flops 2147483648 | bytes 7340032 | tf_op jit(solution)/shard_map/pallas_call | solution.py:229
  116.6 2.7 %collective-permute-start.38 = (bf16[256,128]{1,0:T(8,128)(2,1)S(1)}, bf16[256,128]{1,0:T(8,128)(2,1)S(1)}, u32[]{:S(2)}, u32[]{:S(2)}) collective-permute-start(bf16[256,128]{1,0:T(8,128)(2,1)S(1)} %get-tuple-element.107), channel_id=1, source_target_pairs={{0,4},{4,0},{8,12},{12,8},{16,20},{20,16},{24,28},{28,24},{1,5},{5... | collective-permute-start | bytes 196616 | tf_op jit(solution)/shard_map/ppermute | solution.py:21
  122.0 3.2 %collective-permute-start.42 = (bf16[256,128]{1,0:T(8,128)(2,1)S(1)}, bf16[256,128]{1,0:T(8,128)(2,1)S(1)}, u32[]{:S(2)}, u32[]{:S(2)}) collective-permute-start(bf16[256,128]{1,0:T(8,128)(2,1)S(1)} %get-tuple-element.111), channel_id=1, source_target_pairs={{0,20},{4,16},{8,28},{12,24},{16,4},{20,0},{24,12},{28,8},{1,21},{... | collective-permute-start | bytes 196616 | tf_op jit(solution)/shard_map/ppermute | solution.py:21
  125.9 2.0 %collective-permute-start.43 = (bf16[256,128]{1,0:T(8,128)(2,1)S(1)}, bf16[256,128]{1,0:T(8,128)(2,1)S(1)}, u32[]{:S(2)}, u32[]{:S(2)}) collective-permute-start(bf16[256,128]{1,0:T(8,128)(2,1)S(1)} %get-tuple-element.112), channel_id=1, source_target_pairs={{0,24},{4,28},{8,16},{12,20},{16,8},{20,12},{24,0},{28,4},{1,25},{... | collective-permute-start | bytes 196616 | tf_op jit(solution)/shard_map/ppermute | solution.py:21
  129.9 3.8 %collective-permute-done.42 = bf16[256,128]{1,0:T(8,128)(2,1)S(1)} collective-permute-done((bf16[256,128]{1,0:T(8,128)(2,1)S(1)}, bf16[256,128]{1,0:T(8,128)(2,1)S(1)}, u32[]{:S(2)}, u32[]{:S(2)}) %collective-permute-start.42) | collective-permute-done | bytes 65568 | tf_op jit(solution)/shard_map/ppermute | solution.py:21
  (124 shorter events, 41.3 us)
Async XLA Ops:
  2.3 12.5 %collective-permute-start.25 = (bf16[128,512]{1,0:T(8,128)(2,1)S(1)}, bf16[128,512]{1,0:T(8,128)(2,1)S(1)}, u32[]{:S(2)}, u32[]{:S(2)}) collective-permute-start(bf16[128,512]{1,0:T(8,128)(2,1)S(1)} %get-tuple-element.87), channel_id=1, source_target_pairs={{0,24},{4,28},{8,16},{12,20},{16,8},{20,12},{24,0},{28,4},{1,25},{... | collective-permute-start | bytes 393224 | tf_op jit(solution)/shard_map/ppermute | solution.py:21
  7.4 15.4 %collective-permute-start.26 = (bf16[128,512]{1,0:T(8,128)(2,1)S(1)}, bf16[128,512]{1,0:T(8,128)(2,1)S(1)}, u32[]{:S(2)}, u32[]{:S(2)}) collective-permute-start(bf16[128,512]{1,0:T(8,128)(2,1)S(1)} %get-tuple-element.88), channel_id=1, source_target_pairs={{0,28},{4,24},{8,20},{12,16},{16,12},{20,8},{24,4},{28,0},{1,29},{... | collective-permute-start | bytes 393224 | tf_op jit(solution)/shard_map/ppermute | solution.py:21
  8.6 27.6 %collective-permute-start.15 = (bf16[128,512]{1,0:T(8,128)(2,1)S(1)}, bf16[128,512]{1,0:T(8,128)(2,1)S(1)}, u32[]{:S(2)}, u32[]{:S(2)}) collective-permute-start(bf16[128,512]{1,0:T(8,128)(2,1)S(1)} %get-tuple-element.81), channel_id=1, source_target_pairs={{0,16},{4,20},{8,24},{12,28},{16,0},{20,4},{24,8},{28,12},{1,17},{... | collective-permute-start | bytes 393224 | tf_op jit(solution)/shard_map/ppermute | solution.py:21
  9.4 26.8 %collective-permute-start.16 = (bf16[128,512]{1,0:T(8,128)(2,1)S(1)}, bf16[128,512]{1,0:T(8,128)(2,1)S(1)}, u32[]{:S(2)}, u32[]{:S(2)}) collective-permute-start(bf16[128,512]{1,0:T(8,128)(2,1)S(1)} %get-tuple-element.82), channel_id=1, source_target_pairs={{0,20},{4,16},{8,28},{12,24},{16,4},{20,0},{24,12},{28,8},{1,21},{... | collective-permute-start | bytes 393224 | tf_op jit(solution)/shard_map/ppermute | solution.py:21
  11.3 15.2 %collective-permute-start.3 = (bf16[128,512]{1,0:T(8,128)(2,1)S(1)}, bf16[128,512]{1,0:T(8,128)(2,1)S(1)}, u32[]{:S(2)}, u32[]{:S(2)}) collective-permute-start(bf16[128,512]{1,0:T(8,128)(2,1)S(1)} %get-tuple-element.74), channel_id=1, source_target_pairs={{0,4},{4,0},{8,12},{12,8},{16,20},{20,16},{24,28},{28,24},{1,5},{5... | collective-permute-start | bytes 393224 | tf_op jit(solution)/shard_map/ppermute | solution.py:21
  14.8 17.0 %collective-permute-start.4 = (bf16[128,512]{1,0:T(8,128)(2,1)S(1)}, bf16[128,512]{1,0:T(8,128)(2,1)S(1)}, u32[]{:S(2)}, u32[]{:S(2)}) collective-permute-start(bf16[128,512]{1,0:T(8,128)(2,1)S(1)} %get-tuple-element.75), channel_id=1, source_target_pairs={{0,8},{4,12},{8,0},{12,4},{16,24},{20,28},{24,16},{28,20},{1,9},{5... | collective-permute-start | bytes 393224 | tf_op jit(solution)/shard_map/ppermute | solution.py:21
  22.8 11.7 %collective-permute-start.5 = (bf16[128,512]{1,0:T(8,128)(2,1)S(1)}, bf16[128,512]{1,0:T(8,128)(2,1)S(1)}, u32[]{:S(2)}, u32[]{:S(2)}) collective-permute-start(bf16[128,512]{1,0:T(8,128)(2,1)S(1)} %get-tuple-element.76), channel_id=1, source_target_pairs={{0,12},{4,8},{8,4},{12,0},{16,28},{20,24},{24,20},{28,16},{1,13},{... | collective-permute-start | bytes 393224 | tf_op jit(solution)/shard_map/ppermute | solution.py:21
  26.5 10.2 %collective-permute-start.28 = (bf16[256,512]{1,0:T(8,128)(2,1)S(1)}, bf16[256,512]{1,0:T(8,128)(2,1)S(1)}, u32[]{:S(2)}, u32[]{:S(2)}) collective-permute-start(bf16[256,512]{1,0:T(8,128)(2,1)S(1)} %constant_dynamic-update-slice_fusion.5.refs_0_.refs_12_), channel_id=1, source_target_pairs={{0,2},{1,3},{2,0},{3,1},{4,6},{5,7},{6,4},{7,5},{8,10},{9,11},{10,... | collective-permute-start | bytes 786440 | tf_op jit(solution)/shard_map/ppermute | solution.py:21
  31.7 12.3 %collective-permute-start.27 = (bf16[256,512]{1,0:T(8,128)(2,1)S(1)}, bf16[256,512]{1,0:T(8,128)(2,1)S(1)}, u32[]{:S(2)}, u32[]{:S(2)}) collective-permute-start(bf16[256,512]{1,0:T(8,128)(2,1)S(1)} %constant_dynamic-update-slice_fusion.5.refs_0_.refs_12_), channel_id=1, source_target_pairs={{0,1},{1,0},{2,3},{3,2},{4,5},{5,4},{6,7},{7,6},{8,9},{9,8},{10,11... | collective-permute-start | bytes 786440 | tf_op jit(solution)/shard_map/ppermute | solution.py:21
  34.6 15.6 %collective-permute-start.7 = (bf16[384,512]{1,0:T(8,128)(2,1)S(1)}, bf16[384,512]{1,0:T(8,128)(2,1)S(1)}, u32[]{:S(2)}, u32[]{:S(2)}) collective-permute-start(bf16[384,512]{1,0:T(8,128)(2,1)S(1)} %constant_dynamic-update-slice_fusion.refs_0_.refs_4_), channel_id=1, source_target_pairs={{0,2},{1,3},{2,0},{3,1},{4,6},{5,7},{6,4},{7,5},{8,10},{9,11},{10,... | collective-permute-start | bytes 1179656 | tf_op jit(solution)/shard_map/ppermute | solution.py:21
  36.2 13.9 %collective-permute-start.18 = (bf16[256,512]{1,0:T(8,128)(2,1)S(1)}, bf16[256,512]{1,0:T(8,128)(2,1)S(1)}, u32[]{:S(2)}, u32[]{:S(2)}) collective-permute-start(bf16[256,512]{1,0:T(8,128)(2,1)S(1)} %constant_dynamic-update-slice_fusion.3.refs_0_.refs_8_), channel_id=1, source_target_pairs={{0,2},{1,3},{2,0},{3,1},{4,6},{5,7},{6,4},{7,5},{8,10},{9,11},{10,... | collective-permute-start | bytes 786440 | tf_op jit(solution)/shard_map/ppermute | solution.py:21
  36.8 13.9 %collective-permute-start.29 = (bf16[256,512]{1,0:T(8,128)(2,1)S(1)}, bf16[256,512]{1,0:T(8,128)(2,1)S(1)}, u32[]{:S(2)}, u32[]{:S(2)}) collective-permute-start(bf16[256,512]{1,0:T(8,128)(2,1)S(1)} %collective-permute-done.28.refs_2_.refs_14_), channel_id=1, source_target_pairs={{0,1},{1,0},{2,3},{3,2},{4,5},{5,4},{6,7},{7,6},{8,9},{9,8},{10,11... | collective-permute-start | bytes 786440 | tf_op jit(solution)/shard_map/ppermute | solution.py:21
  52.9 28.5 %collective-permute-start = (bf16[128,512]{1,0:T(8,128)(2,1)S(1)}, bf16[128,512]{1,0:T(8,128)(2,1)S(1)}, u32[]{:S(2)}, u32[]{:S(2)}) collective-permute-start(bf16[128,512]{1,0:T(8,128)(2,1)S(1)} %get-tuple-element.71), channel_id=1, source_target_pairs={{0,1},{1,0},{2,3},{3,2},{4,5},{5,4},{6,7},{7,6},{8,9},{9,8},{10,11... | collective-permute-start | bytes 393224 | tf_op jit(solution)/shard_map/ppermute | solution.py:21
  53.0 32.2 %collective-permute-start.2 = (bf16[128,512]{1,0:T(8,128)(2,1)S(1)}, bf16[128,512]{1,0:T(8,128)(2,1)S(1)}, u32[]{:S(2)}, u32[]{:S(2)}) collective-permute-start(bf16[128,512]{1,0:T(8,128)(2,1)S(1)} %add_convert_fusion.7), channel_id=1, source_target_pairs={{0,2},{1,3},{2,0},{3,1},{4,6},{5,7},{6,4},{7,5},{8,10},{9,11},{10,... | collective-permute-start | bytes 393224 | tf_op jit(solution)/shard_map/ppermute | solution.py:21
  59.9 11.0 %collective-permute-start.22 = (bf16[256,512]{1,0:T(8,128)(2,1)S(1)}, bf16[256,512]{1,0:T(8,128)(2,1)S(1)}, u32[]{:S(2)}, u32[]{:S(2)}) collective-permute-start(bf16[256,512]{1,0:T(8,128)(2,1)S(1)} %add_convert_fusion.5), channel_id=1, source_target_pairs={{0,2},{1,3},{2,0},{3,1},{4,6},{5,7},{6,4},{7,5},{8,10},{9,11},{10,... | collective-permute-start | bytes 786440 | tf_op jit(solution)/shard_map/ppermute | solution.py:21
  68.1 17.8 %collective-permute-start.33 = (bf16[128,512]{1,0:T(8,128)(2,1)S(1)}, bf16[128,512]{1,0:T(8,128)(2,1)S(1)}, u32[]{:S(2)}, u32[]{:S(2)}) collective-permute-start(bf16[128,512]{1,0:T(8,128)(2,1)S(1)} %get-tuple-element.122), channel_id=1, source_target_pairs={{0,24},{4,28},{8,16},{12,20},{16,8},{20,12},{24,0},{28,4},{1,25},{... | collective-permute-start | bytes 393224 | tf_op jit(solution)/shard_map/ppermute | solution.py:21
  70.9 10.3 %collective-permute-start.11 = (bf16[384,512]{1,0:T(8,128)(2,1)S(1)}, bf16[384,512]{1,0:T(8,128)(2,1)S(1)}, u32[]{:S(2)}, u32[]{:S(2)}) collective-permute-start(bf16[384,512]{1,0:T(8,128)(2,1)S(1)} %add_convert_fusion.1), channel_id=1, source_target_pairs={{0,2},{1,3},{2,0},{3,1},{4,6},{5,7},{6,4},{7,5},{8,10},{9,11},{10,... | collective-permute-start | bytes 1179656 | tf_op jit(solution)/shard_map/ppermute | solution.py:21
  71.8 14.1 %collective-permute-start.34 = (bf16[128,512]{1,0:T(8,128)(2,1)S(1)}, bf16[128,512]{1,0:T(8,128)(2,1)S(1)}, u32[]{:S(2)}, u32[]{:S(2)}) collective-permute-start(bf16[128,512]{1,0:T(8,128)(2,1)S(1)} %get-tuple-element.121), channel_id=1, source_target_pairs={{0,28},{4,24},{8,20},{12,16},{16,12},{20,8},{24,4},{28,0},{1,29},{... | collective-permute-start | bytes 393224 | tf_op jit(solution)/shard_map/ppermute | solution.py:21
  81.2 10.7 %collective-permute-start.23 = (bf16[128,512]{1,0:T(8,128)(2,1)S(1)}, bf16[128,512]{1,0:T(8,128)(2,1)S(1)}, u32[]{:S(2)}, u32[]{:S(2)}) collective-permute-start(bf16[128,512]{1,0:T(8,128)(2,1)S(1)} %get-tuple-element.124), channel_id=1, source_target_pairs={{0,16},{4,20},{8,24},{12,28},{16,0},{20,4},{24,8},{28,12},{1,17},{... | collective-permute-start | bytes 393224 | tf_op jit(solution)/shard_map/ppermute | solution.py:21
  81.4 13.0 %collective-permute-start.24 = (bf16[128,512]{1,0:T(8,128)(2,1)S(1)}, bf16[128,512]{1,0:T(8,128)(2,1)S(1)}, u32[]{:S(2)}, u32[]{:S(2)}) collective-permute-start(bf16[128,512]{1,0:T(8,128)(2,1)S(1)} %get-tuple-element.123), channel_id=1, source_target_pairs={{0,20},{4,16},{8,28},{12,24},{16,4},{20,0},{24,12},{28,8},{1,21},{... | collective-permute-start | bytes 393224 | tf_op jit(solution)/shard_map/ppermute | solution.py:21
  85.9 11.8 %collective-permute-start.14 = (bf16[128,512]{1,0:T(8,128)(2,1)S(1)}, bf16[128,512]{1,0:T(8,128)(2,1)S(1)}, u32[]{:S(2)}, u32[]{:S(2)}) collective-permute-start(bf16[128,512]{1,0:T(8,128)(2,1)S(1)} %get-tuple-element.118), channel_id=1, source_target_pairs={{0,12},{4,8},{8,4},{12,0},{16,28},{20,24},{24,20},{28,16},{1,13},{... | collective-permute-start | bytes 393224 | tf_op jit(solution)/shard_map/ppermute | solution.py:21
  99.6 14.3 %collective-permute-start.35 = (bf16[256,512]{1,0:T(8,128)(2,1)S(1)}, bf16[256,512]{1,0:T(8,128)(2,1)S(1)}, u32[]{:S(2)}, u32[]{:S(2)}) collective-permute-start(bf16[256,512]{1,0:T(8,128)(2,1)S(1)} %get-tuple-element.105.refs_0_), channel_id=1, source_target_pairs={{0,1},{1,0},{2,3},{3,2},{4,5},{5,4},{6,7},{7,6},{8,9},{9,8},{10,11... | collective-permute-start | bytes 786440 | tf_op jit(solution)/shard_map/ppermute | solution.py:21
  119.3 10.6 %collective-permute-start.40 = (bf16[256,128]{1,0:T(8,128)(2,1)S(1)}, bf16[256,128]{1,0:T(8,128)(2,1)S(1)}, u32[]{:S(2)}, u32[]{:S(2)}) collective-permute-start(bf16[256,128]{1,0:T(8,128)(2,1)S(1)} %get-tuple-element.109), channel_id=1, source_target_pairs={{0,12},{4,8},{8,4},{12,0},{16,28},{20,24},{24,20},{28,16},{1,13},{... | collective-permute-start | bytes 196616 | tf_op jit(solution)/shard_map/ppermute | solution.py:21
  122.0 11.7 %collective-permute-start.42 = (bf16[256,128]{1,0:T(8,128)(2,1)S(1)}, bf16[256,128]{1,0:T(8,128)(2,1)S(1)}, u32[]{:S(2)}, u32[]{:S(2)}) collective-permute-start(bf16[256,128]{1,0:T(8,128)(2,1)S(1)} %get-tuple-element.111), channel_id=1, source_target_pairs={{0,20},{4,16},{8,28},{12,24},{16,4},{20,0},{24,12},{28,8},{1,21},{... | collective-permute-start | bytes 196616 | tf_op jit(solution)/shard_map/ppermute | solution.py:21
  (32 other events, 287.0 us)
where the time goes:
time: 136 us
  starting transfers between devices  59 us (43%)
  waiting for transfers between devices  45.9 us (34%)
  Pallas kernels  26.8 us (20%)
  other arithmetic  2.72 us (2%)
    ppermute x45, starting transfers between devices, swap(): return lax.ppermute(value, axis, route)  57.7 us
    ppermute x45, waiting for transfers between devices, swap(): return lax.ppermute(value, axis, route)  45.9 us
    pallas_call x10, Pallas kernels, flat_call(): pl.pallas_call(kernel, in_specs=[pl.BlockSpec(memory_space=space)] * len(...  21.8 us
    pallas_call x1, Pallas kernels, body(): pl.pallas_call(functools.partial(pre_kernel, capacity), grid_spec=pltpu.P...  5.03 us
  transfers between devices with their start and end apart: 46, of which 14 were waited for; matrix products, arithmetic and copies ran while one was open for 2% of the time, Pallas kernels for 16%

commit v1 on v0

--- a/solution.py
+++ b/solution.py
@@ -1,4 +1,5 @@
 import functools
+import math
 
 import jax
 import jax.numpy as jnp
@@ -64,7 +65,7 @@
 def dispatch_kernel(experts, direct, ids_in, weights_in, cot_in, *refs):
     blocks, (ids, weights, cot, sems) = refs[:-4], refs[-4:]
     order, _, lane = position(direct)
-    capacity = blocks[0].shape[0] if direct else blocks[0].shape[0] // experts
+    capacity = blocks[-1].shape[0] if direct else blocks[0].shape[0] // experts
     cols = cot.shape[1]
     copies = [
         pltpu.make_async_copy(ids_in, ids, sems.at[0]),
@@ -76,17 +77,19 @@
     copies[0].wait()
     copies[1].wait()
     chosen, scale = routing(ids, weights, experts, capacity, order)
+    chosen = chosen.astype(BF16)
     copies[2].wait()
-    rows = dot(chosen.astype(BF16), cot[...], ((1,), (0,))) * scale
     if direct:
+        rows = (dot(chosen[capacity:], cot[...], ((1,), (0,))) * scale[capacity:]).astype(BF16)
         for k in range(1, experts):
-            blocks[k - 1][...] = rows[k * capacity : (k + 1) * capacity].astype(BF16)
+            blocks[k - 1][...] = rows[(k - 1) * capacity : k * capacity]
     else:
-        blocks[0][...] = rows.astype(BF16)
+        blocks[0][...] = (dot(chosen, cot[...], ((1,), (0,))) * scale).astype(BF16)
 
 
 def local_kernel(lanes, experts, capacity, direct, ids_in, weights_in, cot_in, *refs):
-    select, own_cot, *pieces = refs[:-4]
+    sources, targets = refs[:3], refs[3:6]
+    select, own_cot, *pieces = refs[6:-4]
     ids, weights, cot, sems = refs[-4:]
     order, _, lane = position(direct)
     cols = cot.shape[1] // lanes
@@ -95,7 +98,8 @@
         pltpu.make_async_copy(weights_in, weights, sems.at[1]),
         pltpu.make_async_copy(cot_in, cot, sems.at[2]),
     ]
-    for copy in copies:
+    moves = [pltpu.make_async_copy(u, v, sems.at[3 + i]) for i, (u, v) in enumerate(zip(sources, targets))]
+    for copy in copies + moves:
         copy.start()
     for copy in copies:
         copy.wait()
@@ -107,19 +111,27 @@
         for j in range(lanes):
             rows = dot(first, lane_columns(cot, lane ^ j, cols), ((1,), (0,)))
             pieces[j][...] = (rows * scale[:capacity]).astype(BF16)
-
-
-def pre_kernel(capacity, info, x, w_gate, w_up, hidden, slope, swish):
+    for move in moves:
+        move.wait()
+
+
+def pre_kernel(capacity, half, direct, x_in, w_gate, w_up, hidden, slope, swish, x, sem):
+    order, _, _ = position(direct)
+    rows = x.shape[0]
+    pack = rows // capacity
+    start = pl.multiple_of(((order // pack) ^ half) * rows, rows)
+    copy = pltpu.make_async_copy(x_in.at[pl.ds(start, rows)], x, sem.at[0])
+    copy.start()
+    copy.wait()
     gate = dot(x[...], w_gate[...], ((1,), (0,)))
     up = dot(x[...], w_up[...], ((1,), (0,)))
     sig = jax.nn.sigmoid(gate)
     silu = gate * sig
     deriv = up * sig * (1.0 + gate * (1.0 - sig))
     keep = (silu * up).astype(BF16)
-    pack = x.shape[0] // capacity
     for i in range(pack):
         part = slice(i * capacity, (i + 1) * capacity)
-        place = ((info[0] ^ i) & (pack - 1)) * capacity
+        place = ((order ^ i) & (pack - 1)) * capacity
         spot = pl.ds(pl.multiple_of(place, capacity), capacity)
         hidden[spot, :] = keep[part]
         slope[spot, :] = deriv[part]
@@ -145,31 +157,44 @@
         outs[j][...] = out.astype(BF16)
 
 
-def down_kernel(lanes, count, hidden, *refs):
-    pieces, out = refs[:-1], refs[-1]
+def down_kernel(lanes, places, *refs):
+    count = 1 + max(which for which, _ in places)
+    hidden, pieces, out = refs[:count], refs[count:-1], refs[-1]
     cols = out.shape[1] // lanes
     lane = lax.axis_index("tp")
     for j in range(lanes):
         total = None
-        start = 0
-        for g in range(count):
+        for g, (which, start) in enumerate(places):
             piece = pieces[g * lanes + j]
-            size = piece.shape[0]
-            term = dot(hidden[start : start + size], piece[...], ((0,), (0,)))
+            rows = hidden[which][start : start + piece.shape[0]]
+            term = dot(rows, piece[...], ((0,), (0,)))
             total = term if total is None else total + term
-            start += size
         spot = pl.ds(pl.multiple_of((lane ^ j) * cols, cols), cols)
         out[:, spot] = total.astype(BF16)
 
 
-def gate_up_kernel(capacity, count, direct, x, *refs):
-    grads, (out_gate, out_up) = refs[: 2 * count], refs[2 * count :]
+def conv_kernel(d_sum, following, taps, conv_v, conv_c, d_conv_c, d_conv_v):
+    value = d_sum[...]
+    last = value.shape[0] - 1
+    row = lax.broadcasted_iota(jnp.int32, value.shape, 0)
+    once = jnp.where(row == last, following[0:1], pltpu.roll(value, last, 0))
+    twice = jnp.where(row == last, following[1:2], pltpu.roll(once, last, 0))
+    total = taps[0:1] * twice + taps[1:2] * once + taps[2:3] * value
+    d_conv_c[...] = (total * conv_v[...].astype(F32)).astype(BF16)
+    d_conv_v[...] = (total * conv_c[...].astype(F32)).astype(BF16)
+
+
+def in_vmem(array):
+    return pltpu.VMEM(array.shape, array.dtype)
+
+
+def gate_up_kernel(capacity, members, direct, x, *refs):
+    grads, (out_gate, out_up) = refs[:-2], refs[-2:]
     order, _, _ = position(direct)
     gates, ups = None, None
-    k = 0
-    for g in range(count):
+    for g, ks in enumerate(members):
         gate, up = grads[2 * g], grads[2 * g + 1]
-        for i in range(gate.shape[0] // capacity):
+        for i, k in enumerate(ks):
             spot = pl.ds(pl.multiple_of((order ^ k) * capacity, capacity), capacity)
             part = slice(i * capacity, (i + 1) * capacity)
             rows = x[spot, :]
@@ -177,7 +202,6 @@
             two = dot(rows, up[part], ((0,), (0,)))
             gates = one if gates is None else gates + one
             ups = two if ups is None else ups + two
-            k += 1
     out_gate[...] = gates.astype(BF16)
     out_up[...] = ups.astype(BF16)
 
@@ -214,12 +238,18 @@
     d_sum[...] = total * gate
     size = own.shape[0]
     if direct:
-        for k in range(scratch.shape[0] // size):
-            part = scratch[pl.ds(pl.multiple_of((order ^ k) * size, size), size), :]
-            if k == 0:
-                own[...] = part
-            else:
-                outs[k - 1][...] = part.astype(BF16)
+
+        def part(k):
+            return scratch[pl.ds(pl.multiple_of((order ^ k) * size, size), size), :]
+
+        own[...] = part(0)
+        near, stay, cross = outs[:3], outs[3], outs[4]
+        for k in (1, 2, 3):
+            near[k - 1][...] = part(k).astype(BF16)
+        for i, k in enumerate((4, 6)):
+            spot = slice(i * size, (i + 1) * size)
+            stay[spot] = part(k).astype(BF16)
+            cross[spot] = part(k ^ 1).astype(BF16)
     else:
         own[...] = scratch[pl.ds(pl.multiple_of(me * size, size), size), :]
         outs[0][...] = scratch[...].astype(BF16)
@@ -228,7 +258,10 @@
 def flat_call(kernel, ins, outs, flops, limit, scratch=(), space=pltpu.VMEM):
     return pl.pallas_call(
         kernel,
-        in_specs=[pl.BlockSpec(memory_space=space)] * len(ins),
+        in_specs=[
+            pl.BlockSpec(memory_space=space[i] if isinstance(space, tuple) else space)
+            for i in range(len(ins))
+        ],
         out_specs=[pl.BlockSpec(memory_space=pltpu.VMEM)] * len(outs),
         out_shape=outs,
         scratch_shapes=list(scratch),
@@ -236,7 +269,7 @@
         cost_estimate=pl.CostEstimate(
             flops=flops,
             transcendentals=0,
-            bytes_accessed=sum(a.size * a.dtype.itemsize for a in [*ins, *outs]),
+            bytes_accessed=sum(math.prod(a.shape) * a.dtype.itemsize for a in [*ins, *outs]),
         ),
     )(*ins)
 
@@ -245,15 +278,17 @@
     return jax.ShapeDtypeStruct(shape, dtype)
 
 
-def gather_lanes(own, lanes):
-    distance = lanes // 2
-    have = {0: own}
+def spread(have, lanes, distance):
     while distance >= 1:
         for j in list(have):
             k = j ^ distance
             have[k] = swap(have[j], "tp", distance)
         distance //= 2
     return [have[j] for j in range(lanes)]
+
+
+def gather_lanes(own, lanes):
+    return spread({0: own}, lanes, lanes // 2)
 
 
 def sum_lanes(parts, lanes):
@@ -296,7 +331,6 @@
         raise ValueError("unsupported mesh")
     direct = groups == 8
     me = lax.axis_index("sp")
-    order = me if direct else jnp.zeros_like(me)
     x = expert_inputs[0]
     w_gate, w_up, w_down = gate_weight[0], up_weight[0], down_weight[0]
     members = [[0], [1, 2, 3], [4, 5], [6, 7]] if direct else [list(range(groups))]
@@ -317,10 +351,11 @@
         ],
         space=pltpu.HBM,
     )
-    select, own_cot, *own_pieces = flat_call(
+    w_gate, w_up, w_down, select, own_cot, *own_pieces = flat_call(
         functools.partial(local_kernel, lanes, groups, capacity, direct),
-        in_hbm(ids, factors, cotangent),
-        [struct((tokens, slots), BF16), struct((tokens, cols), BF16)]
+        in_hbm(ids, factors, cotangent, w_gate, w_up, w_down),
+        [in_vmem(w) for w in (w_gate, w_up, w_down)]
+        + [struct((tokens, slots), BF16), struct((tokens, cols), BF16)]
         + ([block] * lanes if direct else []),
         2 * slots * tokens * cols,
         14,
@@ -328,40 +363,23 @@
             pltpu.VMEM(ids.shape, jnp.int32),
             pltpu.VMEM(ids.shape, F32),
             pltpu.VMEM((tokens, model_width), BF16),
-            pltpu.SemaphoreType.DMA((3,)),
+            pltpu.SemaphoreType.DMA((6,)),
         ],
         space=pltpu.HBM,
     )
-    pack = min(groups, 4)
-    span = pl.BlockSpec((pack * capacity, units), lambda k, info: (k, 0))
-    weights = pl.BlockSpec((model_width, units), lambda k, info: (0, 0))
-    hidden, slope, swish = pl.pallas_call(
-        functools.partial(pre_kernel, capacity),
-        grid_spec=pltpu.PrefetchScalarGridSpec(
-            num_scalar_prefetch=1,
-            grid=(groups // pack,),
-            in_specs=[
-                pl.BlockSpec(
-                    (pack * capacity, model_width), lambda k, info: ((info[0] // pack) ^ k, 0)
-                ),
-                weights,
-                weights,
-            ],
-            out_specs=[span] * 3,
-        ),
-        out_shape=[
-            struct((slots, units), BF16),
-            struct((slots, units), F32),
-            struct((slots, units), F32),
-        ],
-        compiler_params=pltpu.CompilerParams(vmem_limit_bytes=20 << 20),
-        cost_estimate=pl.CostEstimate(
-            flops=4 * slots * model_width * units,
-            transcendentals=slots * units,
-            bytes_accessed=12 << 20,
-        ),
-        name="pre",
-    )(order.astype(jnp.int32)[None], *in_hbm(x, w_gate, w_up))
+    half_slots = slots // 2
+    halves = [
+        flat_call(
+            functools.partial(pre_kernel, capacity, h, direct),
+            (*in_hbm(x), w_gate, w_up),
+            [struct((half_slots, units), t) for t in (BF16, F32, F32)],
+            4 * half_slots * model_width * units,
+            12,
+            scratch=[pltpu.VMEM((half_slots, model_width), BF16), pltpu.SemaphoreType.DMA((1,))],
+            space=(pltpu.HBM, pltpu.VMEM, pltpu.VMEM),
+        )
+        for h in range(2)
+    ]
 
     def arrive(ks):
         if not direct:
@@ -380,8 +398,12 @@
     grads, returned = {}, {}
     for g, ks in enumerate(members):
         rows = len(ks) * capacity
+        which, offset = divmod(ks[0] * capacity, half_slots)
+        _, slope, swish = halves[which]
+        if not direct:
+            slope, swish = (jnp.concatenate([h[i] for h in halves]) for i in (1, 2))
         gate, up, *parts = flat_call(
-            functools.partial(mid_kernel, lanes, ks[0] * capacity),
+            functools.partial(mid_kernel, lanes, offset),
             (slope, swish, w_gate, w_up, w_down, *arrived[g]),
             [struct((rows, units), BF16)] * 2 + [struct((rows, cols), BF16)] * lanes,
             6 * rows * model_width * units,
@@ -399,17 +421,19 @@
                 returned[k] = swap(one, "sp", k) if k else one
 
     count = len(members)
+    places = [divmod(ks[0] * capacity, half_slots) for ks in members]
+    hidden = [h[0] for h in halves] if direct else [jnp.concatenate([h[0] for h in halves])]
     flat = [piece for g in range(count) for piece in arrived[g]]
     (grad_down,) = flat_call(
-        functools.partial(down_kernel, lanes, count),
-        (hidden, *flat),
+        functools.partial(down_kernel, lanes, places),
+        (*hidden, *flat),
         [struct((units, model_width), BF16)],
         2 * slots * model_width * units,
         16,
     )
     flat = [grad for g in range(count) for grad in grads[g]]
     grad_gate, grad_up = flat_call(
-        functools.partial(gate_up_kernel, capacity, count, direct),
+        functools.partial(gate_up_kernel, capacity, members, direct),
         (x, *flat),
         [struct((model_width, units), BF16)] * 2,
         4 * slots * model_width * units,
@@ -424,7 +448,8 @@
     )
     pieces = gather_lanes(kept, lanes)
     part = struct((part_rows, channels), BF16)
-    outs = [part] * (groups - 1) if direct else [struct((model_width, channels), BF16)]
+    pair = struct((2 * part_rows, channels), BF16)
+    outs = [part] * 3 + [pair] * 2 if direct else [struct((model_width, channels), BF16)]
     shapes = [
         struct((tokens, channels), BF16),
         struct((tokens, channels), F32),
@@ -441,21 +466,27 @@
     back = [(i, i - 1) for i in range(1, groups)]
     next_rows = lax.ppermute(grad_sum[:2], "sp", back)
     if direct:
+        arrived_terms = [swap(terms[k - 1], "sp", k) for k in (1, 2, 3)]
+        crossed = swap(terms[4], "sp", 1)
+        stay = (terms[3].astype(F32) + crossed.astype(F32)).astype(BF16)
+        for i, k in enumerate((4, 6)):
+            half = stay[i * part_rows : (i + 1) * part_rows]
+            arrived_terms.append(swap(half, "sp", k))
         grad_out_weight = own
-        for k in range(1, groups):
-            term = swap(terms[k - 1], "sp", k)
+        for term in arrived_terms:
             grad_out_weight = grad_out_weight + term.astype(F32)
     else:
         value = terms[0].reshape(groups, part_rows, channels)
         value = lax.all_to_all(value, "sp", split_axis=0, concat_axis=0, tiled=True)
         others = (jnp.arange(groups) != me)[:, None, None]
         grad_out_weight = own + jnp.sum(jnp.where(others, value.astype(F32), 0.0), axis=0)
-    extended = jnp.concatenate([grad_sum, next_rows], axis=0)
-    grad_prod = (
-        conv_taps[0] * extended[2:] + conv_taps[1] * extended[1:-1] + conv_taps[2] * extended[:-2]
-    )
-    grad_conv_c = (grad_prod * conv_v.astype(F32)).astype(BF16)
-    grad_conv_v = (grad_prod * conv_c.astype(F32)).astype(BF16)
+    grad_conv_c, grad_conv_v = flat_call(
+        conv_kernel,
+        (grad_sum, next_rows, conv_taps, conv_v, conv_c),
+        [struct((tokens, channels), BF16)] * 2,
+        8 * tokens * channels,
+        8,
+    )
     return (
         grad_input,
         grad_gate[None],

time: 136 us -> 125 us (0.919)
  starting transfers between devices: 59 us -> 47.9 us
  Pallas kernels: 26.8 us -> 28.9 us
    ppermute x45 -> x44, starting transfers between devices: 57.7 us -> 46.5 us  [swap(): return lax.ppermute(value, axis, route)]
    pallas_call x11 -> x13, Pallas kernels: 26.8 us -> 28.9 us  [flat_call(): pl.pallas_call(kernel, in_specs=[pl.BlockSpec(memory_space=space[i] if is...]
    ppermute x45 -> x44, waiting for transfers between devices: 45.9 us -> 45.4 us  [swap(): return lax.ppermute(value, axis, route)]
  transfers between devices with their start and end apart: 46 -> 45, of which waited for: 14 -> 15; matrix products, arithmetic and copies ran while one was open for 2% -> 1% of each run, Pallas kernels for 16% -> 19%
where the time goes in v1:
time: 125 us
  starting transfers between devices  47.9 us (38%)
  waiting for transfers between devices  45.4 us (36%)
  Pallas kernels  28.9 us (23%)
  other arithmetic  1.41 us (1%)
    ppermute x44, starting transfers between devices, swap(): return lax.ppermute(value, axis, route)  46.5 us
    ppermute x44, waiting for transfers between devices, swap(): return lax.ppermute(value, axis, route)  45.4 us
    pallas_call x13, Pallas kernels, flat_call(): pl.pallas_call(kernel, in_specs=[pl.BlockSpec(memory_space=space[i] if is...  28.9 us
  transfers between devices with their start and end apart: 45, of which 15 were waited for; matrix products, arithmetic and copies ran while one was open for 1% of the time, Pallas kernels for 19%

profile of v1, /device:TPU:0, one launch (start us, length us, event | category | flops | bytes accessed | tf_op | source)
XLA Modules:
  0.0 124.8 jit_solution(8929048865029997273)
XLA Ops:
  2.2 4.1 %collective-permute-start.15 = (bf16[128,512]{1,0:T(8,128)(2,1)S(1)}, bf16[128,512]{1,0:T(8,128)(2,1)S(1)}, u32[]{:S(2)}, u32[]{:S(2)}) collective-permute-start(bf16[128,512]{1,0:T(8,128)(2,1)S(1)} %get-tuple-element.92), channel_id=1, source_target_pairs={{0,16},{4,20},{8,24},{12,28},{16,0},{20,4},{24,8},{28,12},{1,17},{... | collective-permute-start | bytes 393224 | tf_op jit(solution)/shard_map/ppermute | solution.py:22
  7.9 1.8 %collective-permute-start.4 = (bf16[128,512]{1,0:T(8,128)(2,1)S(1)}, bf16[128,512]{1,0:T(8,128)(2,1)S(1)}, u32[]{:S(2)}, u32[]{:S(2)}) collective-permute-start(bf16[128,512]{1,0:T(8,128)(2,1)S(1)} %get-tuple-element.84), channel_id=1, source_target_pairs={{0,8},{4,12},{8,0},{12,4},{16,24},{20,28},{24,16},{28,20},{1,9},{5... | collective-permute-start | bytes 393224 | tf_op jit(solution)/shard_map/ppermute | solution.py:22
  11.1 5.2 %collective-permute-done.15 = bf16[128,512]{1,0:T(8,128)(2,1)S(1)} collective-permute-done((bf16[128,512]{1,0:T(8,128)(2,1)S(1)}, bf16[128,512]{1,0:T(8,128)(2,1)S(1)}, u32[]{:S(2)}, u32[]{:S(2)}) %collective-permute-start.15) | collective-permute-done | bytes 131104 | tf_op jit(solution)/shard_map/ppermute | solution.py:22
  16.3 2.9 %collective-permute-start.25 = (bf16[128,512]{1,0:T(8,128)(2,1)S(1)}, bf16[128,512]{1,0:T(8,128)(2,1)S(1)}, u32[]{:S(2)}, u32[]{:S(2)}) collective-permute-start(bf16[128,512]{1,0:T(8,128)(2,1)S(1)} %get-tuple-element.98), channel_id=1, source_target_pairs={{0,24},{4,28},{8,16},{12,20},{16,8},{20,12},{24,0},{28,4},{1,25},{... | collective-permute-start | bytes 393224 | tf_op jit(solution)/shard_map/ppermute | solution.py:22
  19.3 3.6 %collective-permute-start.26 = (bf16[128,512]{1,0:T(8,128)(2,1)S(1)}, bf16[128,512]{1,0:T(8,128)(2,1)S(1)}, u32[]{:S(2)}, u32[]{:S(2)}) collective-permute-start(bf16[128,512]{1,0:T(8,128)(2,1)S(1)} %get-tuple-element.99), channel_id=1, source_target_pairs={{0,28},{4,24},{8,20},{12,16},{16,12},{20,8},{24,4},{28,0},{1,29},{... | collective-permute-start | bytes 393224 | tf_op jit(solution)/shard_map/ppermute | solution.py:22
  25.2 2.0 %collective-permute-done.26 = bf16[128,512]{1,0:T(8,128)(2,1)S(1)} collective-permute-done((bf16[128,512]{1,0:T(8,128)(2,1)S(1)}, bf16[128,512]{1,0:T(8,128)(2,1)S(1)}, u32[]{:S(2)}, u32[]{:S(2)}) %collective-permute-start.26) | collective-permute-done | bytes 131104 | tf_op jit(solution)/shard_map/ppermute | solution.py:22
  28.8 3.3 %collective-permute-done.18.refs_2_.refs_12_ = bf16[256,512]{1,0:T(8,128)(2,1)S(1)} collective-permute-done((bf16[256,512]{1,0:T(8,128)(2,1)S(1)}, bf16[256,512]{1,0:T(8,128)(2,1)S(1)}, u32[]{:S(2)}, u32[]{:S(2)}) %collective-permute-start.18) | collective-permute-done | bytes 262176 | tf_op jit(solution)/shard_map/ppermute | solution.py:22
  32.1 2.3 %shard_map.188 = (bf16[2048,256]{1,0:T(8,128)(2,1)S(1)}, bf16[2048,256]{1,0:T(8,128)(2,1)S(1)}, bf16[256,2048]{1,0:T(8,128)(2,1)S(1)}, bf16[256,1024]{1,0:T(8,12...) custom-call(s32[2,256]{1,0:T(2,128)} %bitcast.17, ...), custom_call_target="tpu_custom_call" | custom-call | flops 268435456 | bytes 8654848 | tf_op jit(solution)/shard_map/pallas_call | solution.py:259
  34.4 2.9 %shard_map.189 = (bf16[512,256]{1,0:T(8,128)(2,1)S(1)}, f32[512,256]{1,0:T(8,128)S(1)}, f32[512,256]{1,0:T(8,128)S(1)}) custom-call(bf16[1024,2048]{1,0:T(8,128)(2,1)} %bitcast.9, bf16[2048,256]{1,0:T(8,128)(2,1)S(1)} %get-tuple-element.70.w_gate, bf16[2048,256]{1,0:T(8,128)(2,1)S(1)} %get-tuple-element.71.w_up), custom_call_target="tpu_custom_call" | custom-call | flops 1073741824 | bytes 7602176 | tf_op jit(solution)/shard_map/pallas_call | solution.py:259
  37.3 1.6 %shard_map.190 = (bf16[128,256]{1,0:T(8,128)(2,1)S(1)}, bf16[128,256]{1,0:T(8,128)(2,1)S(1)}, bf16[128,512]{1,0:T(8,128)(2,1)S(1)}, bf16[128,512]{1,0:T(8,128)(2...) custom-call(f32[512,256]{1,0:T(8,128)S(1)} %get-tuple-element.72.slope, ...), custom_call_target="tpu_custom_call" | custom-call | flops 402653184 | bytes 5373952 | tf_op jit(solution)/shard_map/pallas_call | solution.py:259
  39.5 2.9 %shard_map.193 = (bf16[512,256]{1,0:T(8,128)(2,1)S(1)}, f32[512,256]{1,0:T(8,128)S(1)}, f32[512,256]{1,0:T(8,128)S(1)}) custom-call(bf16[1024,2048]{1,0:T(8,128)(2,1)} %bitcast.10, bf16[2048,256]{1,0:T(8,128)(2,1)S(1)} %get-tuple-element.70.w_gate, bf16[2048,256]{1,0:T(8,128)(2,1)S(1)} %get-tuple-element.71.w_up), custom_call_target="tpu_custom_call" | custom-call | flops 1073741824 | bytes 7602176 | tf_op jit(solution)/shard_map/pallas_call | solution.py:259
  42.5 2.4 %collective-permute-done.28.refs_2_.refs_16_ = bf16[256,512]{1,0:T(8,128)(2,1)S(1)} collective-permute-done((bf16[256,512]{1,0:T(8,128)(2,1)S(1)}, bf16[256,512]{1,0:T(8,128)(2,1)S(1)}, u32[]{:S(2)}, u32[]{:S(2)}) %collective-permute-start.28) | collective-permute-done | bytes 262176 | tf_op jit(solution)/shard_map/ppermute | solution.py:22
  52.6 2.3 %shard_map.192 = (bf16[384,256]{1,0:T(8,128)(2,1)S(1)}, bf16[384,256]{1,0:T(8,128)(2,1)S(1)}, bf16[384,512]{1,0:T(8,128)(2,1)S(1)}, bf16[384,512]{1,0:T(8,128)(2...) custom-call(f32[512,256]{1,0:T(8,128)S(1)} %get-tuple-element.72.slope, ...), custom_call_target="tpu_custom_call" | custom-call | flops 1207959552 | bytes 7733248 | tf_op jit(solution)/shard_map/pallas_call | solution.py:259
  56.6 4.6 %collective-permute-done.22 = bf16[256,512]{1,0:T(8,128)(2,1)S(1)} collective-permute-done((bf16[256,512]{1,0:T(8,128)(2,1)S(1)}, bf16[256,512]{1,0:T(8,128)(2,1)S(1)}, u32[]{:S(2)}, u32[]{:S(2)}) %collective-permute-start.22) | collective-permute-done | bytes 262176 | tf_op jit(solution)/shard_map/ppermute | solution.py:22
  63.3 2.7 %collective-permute-done.32 = bf16[256,512]{1,0:T(8,128)(2,1)S(1)} collective-permute-done((bf16[256,512]{1,0:T(8,128)(2,1)S(1)}, bf16[256,512]{1,0:T(8,128)(2,1)S(1)}, u32[]{:S(2)}, u32[]{:S(2)}) %collective-permute-start.32) | collective-permute-done | bytes 262176 | tf_op jit(solution)/shard_map/ppermute | solution.py:22
  67.9 8.4 %collective-permute-done.11 = bf16[384,512]{1,0:T(8,128)(2,1)S(1)} collective-permute-done((bf16[384,512]{1,0:T(8,128)(2,1)S(1)}, bf16[384,512]{1,0:T(8,128)(2,1)S(1)}, u32[]{:S(2)}, u32[]{:S(2)}) %collective-permute-start.11) | collective-permute-done | bytes 393248 | tf_op jit(solution)/shard_map/ppermute | solution.py:22
  77.3 4.0 %collective-permute-start.33 = (bf16[128,512]{1,0:T(8,128)(2,1)S(1)}, bf16[128,512]{1,0:T(8,128)(2,1)S(1)}, u32[]{:S(2)}, u32[]{:S(2)}) collective-permute-start(bf16[128,512]{1,0:T(8,128)(2,1)S(1)} %get-tuple-element.132), channel_id=1, source_target_pairs={{0,24},{4,28},{8,16},{12,20},{16,8},{20,12},{24,0},{28,4},{1,25},{... | collective-permute-start | bytes 393224 | tf_op jit(solution)/shard_map/ppermute | solution.py:22
  81.3 2.0 %collective-permute-start.13 = (bf16[128,512]{1,0:T(8,128)(2,1)S(1)}, bf16[128,512]{1,0:T(8,128)(2,1)S(1)}, u32[]{:S(2)}, u32[]{:S(2)}) collective-permute-start(bf16[128,512]{1,0:T(8,128)(2,1)S(1)} %get-tuple-element.129), channel_id=1, source_target_pairs={{0,8},{4,12},{8,0},{12,4},{16,24},{20,28},{24,16},{28,20},{1,9},{5... | collective-permute-start | bytes 393224 | tf_op jit(solution)/shard_map/ppermute | solution.py:22
  85.4 2.8 %collective-permute-done.33.refs_6_ = bf16[128,512]{1,0:T(8,128)(2,1)S(1)} collective-permute-done((bf16[128,512]{1,0:T(8,128)(2,1)S(1)}, bf16[128,512]{1,0:T(8,128)(2,1)S(1)}, u32[]{:S(2)}, u32[]{:S(2)}) %collective-permute-start.33) | collective-permute-done | bytes 131104 | tf_op jit(solution)/shard_map/ppermute | solution.py:22
  93.2 7.0 %collective-permute-done.36.refs_2_ = bf16[256,512]{1,0:T(8,128)(2,1)S(1)} collective-permute-done((bf16[256,512]{1,0:T(8,128)(2,1)S(1)}, bf16[256,512]{1,0:T(8,128)(2,1)S(1)}, u32[]{:S(2)}, u32[]{:S(2)}) %collective-permute-start.36) | collective-permute-done | bytes 262176 | tf_op jit(solution)/shard_map/ppermute | solution.py:22
  103.4 5.9 %shard_map.197 = (bf16[2048,256]{1,0:T(8,128)(2,1)}, bf16[2048,256]{1,0:T(8,128)(2,1)}) custom-call(bf16[1024,2048]{1,0:T(8,128)(2,1)S(1)} %bitcast.11, bf16[128,256]{1,0:T(8,128)(2,1)S(1)} %get-tuple-element.105.refs_0_, bf16[128,256]{1,0:T(8,128)(2,1)S(1)} %get-tuple-element.106.refs_1_, bf16[384,256]{1,0:T(8,128)(2,1)S(1)} %get-tuple-element.107.refs_2_, ...), custom_call_target="tpu_custom_call" | custom-call | flops 2147483648 | bytes 7340032 | tf_op jit(solution)/shard_map/pallas_call | solution.py:259
  110.8 2.7 %collective-permute-start.38 = (bf16[256,128]{1,0:T(8,128)(2,1)S(1)}, bf16[256,128]{1,0:T(8,128)(2,1)S(1)}, u32[]{:S(2)}, u32[]{:S(2)}) collective-permute-start(bf16[256,128]{1,0:T(8,128)(2,1)S(1)} %get-tuple-element.119), channel_id=1, source_target_pairs={{0,4},{4,0},{8,12},{12,8},{16,20},{20,16},{24,28},{28,24},{1,5},{5... | collective-permute-start | bytes 196616 | tf_op jit(solution)/shard_map/ppermute | solution.py:22
  117.5 3.4 %collective-permute-start.43 = (bf16[256,128]{1,0:T(8,128)(2,1)S(1)}, bf16[256,128]{1,0:T(8,128)(2,1)S(1)}, u32[]{:S(2)}, u32[]{:S(2)}) collective-permute-start(bf16[256,128]{1,0:T(8,128)(2,1)S(1)} %get-tuple-element.136), channel_id=1, source_target_pairs={{0,24},{4,28},{8,16},{12,20},{16,8},{20,12},{24,0},{28,4},{1,25},{... | collective-permute-start | bytes 196616 | tf_op jit(solution)/shard_map/ppermute | solution.py:22
  120.8 2.5 %shard_map.198 = bf16[256,2048]{1,0:T(8,128)(2,1)} custom-call(bf16[512,256]{1,0:T(8,128)(2,1)S(1)} %get-tuple-element.115.refs_0_, bf16[512,256]{1,0:T(8,128)(2,1)S(1)} %get-tuple-element.116.refs_1_, bf16[128,512]{1,0:T(8,128)(2,1)S(1)} %get-tuple-element.75.refs_0_.refs_2_, bf16[128,512]{1,0:T(8,128)(2,1)S(1)} %get-tuple-element.76.refs_1_.refs_3_, ...), custom_call_target="tpu_custom_call" | custom-call | flops 1073741824 | bytes 5767168 | tf_op jit(solution)/shard_map/pallas_call | solution.py:259
  (115 shorter events, 40.5 us)
Async XLA Ops:
  2.2 14.1 %collective-permute-start.15 = (bf16[128,512]{1,0:T(8,128)(2,1)S(1)}, bf16[128,512]{1,0:T(8,128)(2,1)S(1)}, u32[]{:S(2)}, u32[]{:S(2)}) collective-permute-start(bf16[128,512]{1,0:T(8,128)(2,1)S(1)} %get-tuple-element.92), channel_id=1, source_target_pairs={{0,16},{4,20},{8,24},{12,28},{16,0},{20,4},{24,8},{28,12},{1,17},{... | collective-permute-start | bytes 393224 | tf_op jit(solution)/shard_map/ppermute | solution.py:22
  6.3 12.9 %collective-permute-start.16 = (bf16[128,512]{1,0:T(8,128)(2,1)S(1)}, bf16[128,512]{1,0:T(8,128)(2,1)S(1)}, u32[]{:S(2)}, u32[]{:S(2)}) collective-permute-start(bf16[128,512]{1,0:T(8,128)(2,1)S(1)} %get-tuple-element.93), channel_id=1, source_target_pairs={{0,20},{4,16},{8,28},{12,24},{16,4},{20,0},{24,12},{28,8},{1,21},{... | collective-permute-start | bytes 393224 | tf_op jit(solution)/shard_map/ppermute | solution.py:22
  7.6 15.3 %collective-permute-start.3 = (bf16[128,512]{1,0:T(8,128)(2,1)S(1)}, bf16[128,512]{1,0:T(8,128)(2,1)S(1)}, u32[]{:S(2)}, u32[]{:S(2)}) collective-permute-start(bf16[128,512]{1,0:T(8,128)(2,1)S(1)} %get-tuple-element.83), channel_id=1, source_target_pairs={{0,4},{4,0},{8,12},{12,8},{16,20},{20,16},{24,28},{28,24},{1,5},{5... | collective-permute-start | bytes 393224 | tf_op jit(solution)/shard_map/ppermute | solution.py:22
  7.9 16.6 %collective-permute-start.4 = (bf16[128,512]{1,0:T(8,128)(2,1)S(1)}, bf16[128,512]{1,0:T(8,128)(2,1)S(1)}, u32[]{:S(2)}, u32[]{:S(2)}) collective-permute-start(bf16[128,512]{1,0:T(8,128)(2,1)S(1)} %get-tuple-element.84), channel_id=1, source_target_pairs={{0,8},{4,12},{8,0},{12,4},{16,24},{20,28},{24,16},{28,20},{1,9},{5... | collective-permute-start | bytes 393224 | tf_op jit(solution)/shard_map/ppermute | solution.py:22
  9.7 14.9 %collective-permute-start.5 = (bf16[128,512]{1,0:T(8,128)(2,1)S(1)}, bf16[128,512]{1,0:T(8,128)(2,1)S(1)}, u32[]{:S(2)}, u32[]{:S(2)}) collective-permute-start(bf16[128,512]{1,0:T(8,128)(2,1)S(1)} %get-tuple-element.85), channel_id=1, source_target_pairs={{0,12},{4,8},{8,4},{12,0},{16,28},{20,24},{24,20},{28,16},{1,13},{... | collective-permute-start | bytes 393224 | tf_op jit(solution)/shard_map/ppermute | solution.py:22
  22.9 9.2 %collective-permute-start.18 = (bf16[256,512]{1,0:T(8,128)(2,1)S(1)}, bf16[256,512]{1,0:T(8,128)(2,1)S(1)}, u32[]{:S(2)}, u32[]{:S(2)}) collective-permute-start(bf16[256,512]{1,0:T(8,128)(2,1)S(1)} %constant_dynamic-update-slice_fusion.3.refs_0_.refs_10_), channel_id=1, source_target_pairs={{0,2},{1,3},{2,0},{3,1},{4,6},{5,7},{6,4},{7,5},{8,10},{9,11},{10,... | collective-permute-start | bytes 786440 | tf_op jit(solution)/shard_map/ppermute | solution.py:22
  24.5 20.4 %collective-permute-start.17 = (bf16[256,512]{1,0:T(8,128)(2,1)S(1)}, bf16[256,512]{1,0:T(8,128)(2,1)S(1)}, u32[]{:S(2)}, u32[]{:S(2)}) collective-permute-start(bf16[256,512]{1,0:T(8,128)(2,1)S(1)} %constant_dynamic-update-slice_fusion.3.refs_0_.refs_10_), channel_id=1, source_target_pairs={{0,1},{1,0},{2,3},{3,2},{4,5},{5,4},{6,7},{7,6},{8,9},{9,8},{10,11... | collective-permute-start | bytes 786440 | tf_op jit(solution)/shard_map/ppermute | solution.py:22
  24.6 20.7 %collective-permute-start.7 = (bf16[384,512]{1,0:T(8,128)(2,1)S(1)}, bf16[384,512]{1,0:T(8,128)(2,1)S(1)}, u32[]{:S(2)}, u32[]{:S(2)}) collective-permute-start(bf16[384,512]{1,0:T(8,128)(2,1)S(1)} %constant_dynamic-update-slice_fusion.refs_0_.refs_6_), channel_id=1, source_target_pairs={{0,2},{1,3},{2,0},{3,1},{4,6},{5,7},{6,4},{7,5},{8,10},{9,11},{10,... | collective-permute-start | bytes 1179656 | tf_op jit(solution)/shard_map/ppermute | solution.py:22
  27.2 17.6 %collective-permute-start.28 = (bf16[256,512]{1,0:T(8,128)(2,1)S(1)}, bf16[256,512]{1,0:T(8,128)(2,1)S(1)}, u32[]{:S(2)}, u32[]{:S(2)}) collective-permute-start(bf16[256,512]{1,0:T(8,128)(2,1)S(1)} %constant_dynamic-update-slice_fusion.5.refs_0_.refs_14_), channel_id=1, source_target_pairs={{0,2},{1,3},{2,0},{3,1},{4,6},{5,7},{6,4},{7,5},{8,10},{9,11},{10,... | collective-permute-start | bytes 786440 | tf_op jit(solution)/shard_map/ppermute | solution.py:22
  32.1 13.3 %collective-permute-start.19 = (bf16[256,512]{1,0:T(8,128)(2,1)S(1)}, bf16[256,512]{1,0:T(8,128)(2,1)S(1)}, u32[]{:S(2)}, u32[]{:S(2)}) collective-permute-start(bf16[256,512]{1,0:T(8,128)(2,1)S(1)} %collective-permute-done.18.refs_2_.refs_12_), channel_id=1, source_target_pairs={{0,1},{1,0},{2,3},{3,2},{4,5},{5,4},{6,7},{7,6},{8,9},{9,8},{10,11... | collective-permute-start | bytes 786440 | tf_op jit(solution)/shard_map/ppermute | solution.py:22
  47.7 29.6 %collective-permute-start = (bf16[128,512]{1,0:T(8,128)(2,1)S(1)}, bf16[128,512]{1,0:T(8,128)(2,1)S(1)}, u32[]{:S(2)}, u32[]{:S(2)}) collective-permute-start(bf16[128,512]{1,0:T(8,128)(2,1)S(1)} %get-tuple-element.80), channel_id=1, source_target_pairs={{0,1},{1,0},{2,3},{3,2},{4,5},{5,4},{6,7},{7,6},{8,9},{9,8},{10,11... | collective-permute-start | bytes 393224 | tf_op jit(solution)/shard_map/ppermute | solution.py:22
  48.2 33.1 %collective-permute-start.2 = (bf16[128,512]{1,0:T(8,128)(2,1)S(1)}, bf16[128,512]{1,0:T(8,128)(2,1)S(1)}, u32[]{:S(2)}, u32[]{:S(2)}) collective-permute-start(bf16[128,512]{1,0:T(8,128)(2,1)S(1)} %add_convert_fusion.8), channel_id=1, source_target_pairs={{0,2},{1,3},{2,0},{3,1},{4,6},{5,7},{6,4},{7,5},{8,10},{9,11},{10,... | collective-permute-start | bytes 393224 | tf_op jit(solution)/shard_map/ppermute | solution.py:22
  52.1 9.2 %collective-permute-start.22 = (bf16[256,512]{1,0:T(8,128)(2,1)S(1)}, bf16[256,512]{1,0:T(8,128)(2,1)S(1)}, u32[]{:S(2)}, u32[]{:S(2)}) collective-permute-start(bf16[256,512]{1,0:T(8,128)(2,1)S(1)} %add_convert_fusion.5), channel_id=1, source_target_pairs={{0,2},{1,3},{2,0},{3,1},{4,6},{5,7},{6,4},{7,5},{8,10},{9,11},{10,... | collective-permute-start | bytes 786440 | tf_op jit(solution)/shard_map/ppermute | solution.py:22
  55.0 11.0 %collective-permute-start.32 = (bf16[256,512]{1,0:T(8,128)(2,1)S(1)}, bf16[256,512]{1,0:T(8,128)(2,1)S(1)}, u32[]{:S(2)}, u32[]{:S(2)}) collective-permute-start(bf16[256,512]{1,0:T(8,128)(2,1)S(1)} %add_convert_fusion.3), channel_id=1, source_target_pairs={{0,2},{1,3},{2,0},{3,1},{4,6},{5,7},{6,4},{7,5},{8,10},{9,11},{10,... | collective-permute-start | bytes 786440 | tf_op jit(solution)/shard_map/ppermute | solution.py:22
  63.2 18.0 %collective-permute-start.24 = (bf16[128,512]{1,0:T(8,128)(2,1)S(1)}, bf16[128,512]{1,0:T(8,128)(2,1)S(1)}, u32[]{:S(2)}, u32[]{:S(2)}) collective-permute-start(bf16[128,512]{1,0:T(8,128)(2,1)S(1)} %get-tuple-element.133), channel_id=1, source_target_pairs={{0,20},{4,16},{8,28},{12,24},{16,4},{20,0},{24,12},{28,8},{1,21},{... | collective-permute-start | bytes 393224 | tf_op jit(solution)/shard_map/ppermute | solution.py:22
  66.0 10.2 %collective-permute-start.11 = (bf16[384,512]{1,0:T(8,128)(2,1)S(1)}, bf16[384,512]{1,0:T(8,128)(2,1)S(1)}, u32[]{:S(2)}, u32[]{:S(2)}) collective-permute-start(bf16[384,512]{1,0:T(8,128)(2,1)S(1)} %add_convert_fusion.1), channel_id=1, source_target_pairs={{0,2},{1,3},{2,0},{3,1},{4,6},{5,7},{6,4},{7,5},{8,10},{9,11},{10,... | collective-permute-start | bytes 1179656 | tf_op jit(solution)/shard_map/ppermute | solution.py:22
  66.6 16.6 %collective-permute-start.23 = (bf16[128,512]{1,0:T(8,128)(2,1)S(1)}, bf16[128,512]{1,0:T(8,128)(2,1)S(1)}, u32[]{:S(2)}, u32[]{:S(2)}) collective-permute-start(bf16[128,512]{1,0:T(8,128)(2,1)S(1)} %get-tuple-element.134), channel_id=1, source_target_pairs={{0,16},{4,20},{8,24},{12,28},{16,0},{20,4},{24,8},{28,12},{1,17},{... | collective-permute-start | bytes 393224 | tf_op jit(solution)/shard_map/ppermute | solution.py:22
  76.2 9.1 %collective-permute-start.34 = (bf16[128,512]{1,0:T(8,128)(2,1)S(1)}, bf16[128,512]{1,0:T(8,128)(2,1)S(1)}, u32[]{:S(2)}, u32[]{:S(2)}) collective-permute-start(bf16[128,512]{1,0:T(8,128)(2,1)S(1)} %get-tuple-element.131), channel_id=1, source_target_pairs={{0,28},{4,24},{8,20},{12,16},{16,12},{20,8},{24,4},{28,0},{1,29},{... | collective-permute-start | bytes 393224 | tf_op jit(solution)/shard_map/ppermute | solution.py:22
  77.3 10.9 %collective-permute-start.33 = (bf16[128,512]{1,0:T(8,128)(2,1)S(1)}, bf16[128,512]{1,0:T(8,128)(2,1)S(1)}, u32[]{:S(2)}, u32[]{:S(2)}) collective-permute-start(bf16[128,512]{1,0:T(8,128)(2,1)S(1)} %get-tuple-element.132), channel_id=1, source_target_pairs={{0,24},{4,28},{8,16},{12,20},{16,8},{20,12},{24,0},{28,4},{1,25},{... | collective-permute-start | bytes 393224 | tf_op jit(solution)/shard_map/ppermute | solution.py:22
  81.3 10.0 %collective-permute-start.13 = (bf16[128,512]{1,0:T(8,128)(2,1)S(1)}, bf16[128,512]{1,0:T(8,128)(2,1)S(1)}, u32[]{:S(2)}, u32[]{:S(2)}) collective-permute-start(bf16[128,512]{1,0:T(8,128)(2,1)S(1)} %get-tuple-element.129), channel_id=1, source_target_pairs={{0,8},{4,12},{8,0},{12,4},{16,24},{20,28},{24,16},{28,20},{1,9},{5... | collective-permute-start | bytes 393224 | tf_op jit(solution)/shard_map/ppermute | solution.py:22
  103.4 13.0 %collective-permute-start.41 = (bf16[512,128]{1,0:T(8,128)(2,1)S(1)}, bf16[512,128]{1,0:T(8,128)(2,1)S(1)}, u32[]{:S(2)}, u32[]{:S(2)}) collective-permute-start(bf16[512,128]{1,0:T(8,128)(2,1)S(1)} %get-tuple-element.123), channel_id=1, source_target_pairs={{0,4},{4,0},{8,12},{12,8},{16,20},{20,16},{24,28},{28,24},{1,5},{5... | collective-permute-start | bytes 393224 | tf_op jit(solution)/shard_map/ppermute | solution.py:22
  110.8 13.3 %collective-permute-start.38 = (bf16[256,128]{1,0:T(8,128)(2,1)S(1)}, bf16[256,128]{1,0:T(8,128)(2,1)S(1)}, u32[]{:S(2)}, u32[]{:S(2)}) collective-permute-start(bf16[256,128]{1,0:T(8,128)(2,1)S(1)} %get-tuple-element.119), channel_id=1, source_target_pairs={{0,4},{4,0},{8,12},{12,8},{16,20},{20,16},{24,28},{28,24},{1,5},{5... | collective-permute-start | bytes 196616 | tf_op jit(solution)/shard_map/ppermute | solution.py:22
  113.5 10.6 %collective-permute-start.39 = (bf16[256,128]{1,0:T(8,128)(2,1)S(1)}, bf16[256,128]{1,0:T(8,128)(2,1)S(1)}, u32[]{:S(2)}, u32[]{:S(2)}) collective-permute-start(bf16[256,128]{1,0:T(8,128)(2,1)S(1)} %get-tuple-element.120), channel_id=1, source_target_pairs={{0,8},{4,12},{8,0},{12,4},{16,24},{20,28},{24,16},{28,20},{1,9},{5... | collective-permute-start | bytes 196616 | tf_op jit(solution)/shard_map/ppermute | solution.py:22
  114.9 9.1 %collective-permute-start.40 = (bf16[256,128]{1,0:T(8,128)(2,1)S(1)}, bf16[256,128]{1,0:T(8,128)(2,1)S(1)}, u32[]{:S(2)}, u32[]{:S(2)}) collective-permute-start(bf16[256,128]{1,0:T(8,128)(2,1)S(1)} %get-tuple-element.121), channel_id=1, source_target_pairs={{0,12},{4,8},{8,4},{12,0},{16,28},{20,24},{24,20},{28,16},{1,13},{... | collective-permute-start | bytes 196616 | tf_op jit(solution)/shard_map/ppermute | solution.py:22
  (28 other events, 327.6 us)

commit v2 on v1

--- a/solution.py
+++ b/solution.py
@@ -191,19 +191,27 @@
 def gate_up_kernel(capacity, members, direct, x, *refs):
     grads, (out_gate, out_up) = refs[:-2], refs[-2:]
     order, _, _ = position(direct)
-    gates, ups = None, None
+    gates, ups = {}, {}
     for g, ks in enumerate(members):
-        gate, up = grads[2 * g], grads[2 * g + 1]
         for i, k in enumerate(ks):
-            spot = pl.ds(pl.multiple_of((order ^ k) * capacity, capacity), capacity)
             part = slice(i * capacity, (i + 1) * capacity)
-            rows = x[spot, :]
-            one = dot(rows, gate[part], ((0,), (0,)))
-            two = dot(rows, up[part], ((0,), (0,)))
-            gates = one if gates is None else gates + one
-            ups = two if ups is None else ups + two
-    out_gate[...] = gates.astype(BF16)
-    out_up[...] = ups.astype(BF16)
+            gates[k] = grads[2 * g][part]
+            ups[k] = grads[2 * g + 1][part]
+
+    def paired(values, k):
+        low, high = values[k], values[k + 1]
+        if not direct:
+            return jnp.concatenate([low, high], axis=0)
+        odd = (order & 1) == 1
+        return jnp.concatenate([jnp.where(odd, high, low), jnp.where(odd, low, high)], axis=0)
+
+    for values, out in ((gates, out_gate), (ups, out_up)):
+        total = None
+        for k in range(0, len(values), 2):
+            start = pl.multiple_of(((order // 2) ^ (k // 2)) * 2 * capacity, 2 * capacity)
+            term = dot(x[pl.ds(start, 2 * capacity), :], paired(values, k), ((0,), (0,)))
+            total = term if total is None else total + term
+        out[...] = total.astype(BF16)
 
 
 def combine_kernel(select, cot, *refs):

time: 125 us -> 123 us (0.984)
  Pallas kernels: 28.9 us -> 26.7 us
    pallas_call x13, Pallas kernels: 28.9 us -> 26.7 us  [flat_call(): pl.pallas_call(kernel, in_specs=[pl.BlockSpec(memory_space=space[i] if is...]
  transfers between devices with their start and end apart: 45 -> 45, of which waited for: 15 -> 15; matrix products, arithmetic and copies ran while one was open for 1% -> 1% of each run, Pallas kernels for 19% -> 18%
where the time goes in v2:
time: 123 us
  starting transfers between devices  47.9 us (39%)
  waiting for transfers between devices  45.4 us (37%)
  Pallas kernels  26.7 us (22%)
  other arithmetic  1.41 us (1%)
    ppermute x44, starting transfers between devices, swap(): return lax.ppermute(value, axis, route)  46.5 us
    ppermute x44, waiting for transfers between devices, swap(): return lax.ppermute(value, axis, route)  45.4 us
    pallas_call x13, Pallas kernels, flat_call(): pl.pallas_call(kernel, in_specs=[pl.BlockSpec(memory_space=space[i] if is...  26.7 us
  transfers between devices with their start and end apart: 45, of which 15 were waited for; matrix products, arithmetic and copies ran while one was open for 1% of the time, Pallas kernels for 18%

profile of v2, /device:TPU:0, one launch (start us, length us, event | category | flops | bytes accessed | tf_op | source)
XLA Modules:
  0.0 122.7 jit_solution(4590463669857869781)
XLA Ops:
  2.2 4.1 %collective-permute-start.15 = (bf16[128,512]{1,0:T(8,128)(2,1)S(1)}, bf16[128,512]{1,0:T(8,128)(2,1)S(1)}, u32[]{:S(2)}, u32[]{:S(2)}) collective-permute-start(bf16[128,512]{1,0:T(8,128)(2,1)S(1)} %get-tuple-element.92), channel_id=1, source_target_pairs={{0,16},{4,20},{8,24},{12,28},{16,0},{20,4},{24,8},{28,12},{1,17},{... | collective-permute-start | bytes 393224 | tf_op jit(solution)/shard_map/ppermute | solution.py:22
  7.9 1.8 %collective-permute-start.4 = (bf16[128,512]{1,0:T(8,128)(2,1)S(1)}, bf16[128,512]{1,0:T(8,128)(2,1)S(1)}, u32[]{:S(2)}, u32[]{:S(2)}) collective-permute-start(bf16[128,512]{1,0:T(8,128)(2,1)S(1)} %get-tuple-element.84), channel_id=1, source_target_pairs={{0,8},{4,12},{8,0},{12,4},{16,24},{20,28},{24,16},{28,20},{1,9},{5... | collective-permute-start | bytes 393224 | tf_op jit(solution)/shard_map/ppermute | solution.py:22
  11.1 5.2 %collective-permute-done.15 = bf16[128,512]{1,0:T(8,128)(2,1)S(1)} collective-permute-done((bf16[128,512]{1,0:T(8,128)(2,1)S(1)}, bf16[128,512]{1,0:T(8,128)(2,1)S(1)}, u32[]{:S(2)}, u32[]{:S(2)}) %collective-permute-start.15) | collective-permute-done | bytes 131104 | tf_op jit(solution)/shard_map/ppermute | solution.py:22
  16.3 2.9 %collective-permute-start.25 = (bf16[128,512]{1,0:T(8,128)(2,1)S(1)}, bf16[128,512]{1,0:T(8,128)(2,1)S(1)}, u32[]{:S(2)}, u32[]{:S(2)}) collective-permute-start(bf16[128,512]{1,0:T(8,128)(2,1)S(1)} %get-tuple-element.98), channel_id=1, source_target_pairs={{0,24},{4,28},{8,16},{12,20},{16,8},{20,12},{24,0},{28,4},{1,25},{... | collective-permute-start | bytes 393224 | tf_op jit(solution)/shard_map/ppermute | solution.py:22
  19.3 3.6 %collective-permute-start.26 = (bf16[128,512]{1,0:T(8,128)(2,1)S(1)}, bf16[128,512]{1,0:T(8,128)(2,1)S(1)}, u32[]{:S(2)}, u32[]{:S(2)}) collective-permute-start(bf16[128,512]{1,0:T(8,128)(2,1)S(1)} %get-tuple-element.99), channel_id=1, source_target_pairs={{0,28},{4,24},{8,20},{12,16},{16,12},{20,8},{24,4},{28,0},{1,29},{... | collective-permute-start | bytes 393224 | tf_op jit(solution)/shard_map/ppermute | solution.py:22
  25.2 2.0 %collective-permute-done.26 = bf16[128,512]{1,0:T(8,128)(2,1)S(1)} collective-permute-done((bf16[128,512]{1,0:T(8,128)(2,1)S(1)}, bf16[128,512]{1,0:T(8,128)(2,1)S(1)}, u32[]{:S(2)}, u32[]{:S(2)}) %collective-permute-start.26) | collective-permute-done | bytes 131104 | tf_op jit(solution)/shard_map/ppermute | solution.py:22
  28.8 3.3 %collective-permute-done.18.refs_2_.refs_12_ = bf16[256,512]{1,0:T(8,128)(2,1)S(1)} collective-permute-done((bf16[256,512]{1,0:T(8,128)(2,1)S(1)}, bf16[256,512]{1,0:T(8,128)(2,1)S(1)}, u32[]{:S(2)}, u32[]{:S(2)}) %collective-permute-start.18) | collective-permute-done | bytes 262176 | tf_op jit(solution)/shard_map/ppermute | solution.py:22
  32.1 2.3 %shard_map.188 = (bf16[2048,256]{1,0:T(8,128)(2,1)S(1)}, bf16[2048,256]{1,0:T(8,128)(2,1)S(1)}, bf16[256,2048]{1,0:T(8,128)(2,1)S(1)}, bf16[256,1024]{1,0:T(8,12...) custom-call(s32[2,256]{1,0:T(2,128)} %bitcast.17, ...), custom_call_target="tpu_custom_call" | custom-call | flops 268435456 | bytes 8654848 | tf_op jit(solution)/shard_map/pallas_call | solution.py:267
  34.4 2.9 %shard_map.189 = (bf16[512,256]{1,0:T(8,128)(2,1)S(1)}, f32[512,256]{1,0:T(8,128)S(1)}, f32[512,256]{1,0:T(8,128)S(1)}) custom-call(bf16[1024,2048]{1,0:T(8,128)(2,1)} %bitcast.9, bf16[2048,256]{1,0:T(8,128)(2,1)S(1)} %get-tuple-element.70.w_gate, bf16[2048,256]{1,0:T(8,128)(2,1)S(1)} %get-tuple-element.71.w_up), custom_call_target="tpu_custom_call" | custom-call | flops 1073741824 | bytes 7602176 | tf_op jit(solution)/shard_map/pallas_call | solution.py:267
  37.3 1.6 %shard_map.190 = (bf16[128,256]{1,0:T(8,128)(2,1)S(1)}, bf16[128,256]{1,0:T(8,128)(2,1)S(1)}, bf16[128,512]{1,0:T(8,128)(2,1)S(1)}, bf16[128,512]{1,0:T(8,128)(2...) custom-call(f32[512,256]{1,0:T(8,128)S(1)} %get-tuple-element.72.slope, ...), custom_call_target="tpu_custom_call" | custom-call | flops 402653184 | bytes 5373952 | tf_op jit(solution)/shard_map/pallas_call | solution.py:267
  39.5 2.9 %shard_map.193 = (bf16[512,256]{1,0:T(8,128)(2,1)S(1)}, f32[512,256]{1,0:T(8,128)S(1)}, f32[512,256]{1,0:T(8,128)S(1)}) custom-call(bf16[1024,2048]{1,0:T(8,128)(2,1)} %bitcast.10, bf16[2048,256]{1,0:T(8,128)(2,1)S(1)} %get-tuple-element.70.w_gate, bf16[2048,256]{1,0:T(8,128)(2,1)S(1)} %get-tuple-element.71.w_up), custom_call_target="tpu_custom_call" | custom-call | flops 1073741824 | bytes 7602176 | tf_op jit(solution)/shard_map/pallas_call | solution.py:267
  42.5 2.4 %collective-permute-done.28.refs_2_.refs_16_ = bf16[256,512]{1,0:T(8,128)(2,1)S(1)} collective-permute-done((bf16[256,512]{1,0:T(8,128)(2,1)S(1)}, bf16[256,512]{1,0:T(8,128)(2,1)S(1)}, u32[]{:S(2)}, u32[]{:S(2)}) %collective-permute-start.28) | collective-permute-done | bytes 262176 | tf_op jit(solution)/shard_map/ppermute | solution.py:22
  52.6 2.3 %shard_map.192 = (bf16[384,256]{1,0:T(8,128)(2,1)S(1)}, bf16[384,256]{1,0:T(8,128)(2,1)S(1)}, bf16[384,512]{1,0:T(8,128)(2,1)S(1)}, bf16[384,512]{1,0:T(8,128)(2...) custom-call(f32[512,256]{1,0:T(8,128)S(1)} %get-tuple-element.72.slope, ...), custom_call_target="tpu_custom_call" | custom-call | flops 1207959552 | bytes 7733248 | tf_op jit(solution)/shard_map/pallas_call | solution.py:267
  56.6 4.6 %collective-permute-done.22 = bf16[256,512]{1,0:T(8,128)(2,1)S(1)} collective-permute-done((bf16[256,512]{1,0:T(8,128)(2,1)S(1)}, bf16[256,512]{1,0:T(8,128)(2,1)S(1)}, u32[]{:S(2)}, u32[]{:S(2)}) %collective-permute-start.22) | collective-permute-done | bytes 262176 | tf_op jit(solution)/shard_map/ppermute | solution.py:22
  63.3 2.7 %collective-permute-done.32 = bf16[256,512]{1,0:T(8,128)(2,1)S(1)} collective-permute-done((bf16[256,512]{1,0:T(8,128)(2,1)S(1)}, bf16[256,512]{1,0:T(8,128)(2,1)S(1)}, u32[]{:S(2)}, u32[]{:S(2)}) %collective-permute-start.32) | collective-permute-done | bytes 262176 | tf_op jit(solution)/shard_map/ppermute | solution.py:22
  67.9 8.4 %collective-permute-done.11 = bf16[384,512]{1,0:T(8,128)(2,1)S(1)} collective-permute-done((bf16[384,512]{1,0:T(8,128)(2,1)S(1)}, bf16[384,512]{1,0:T(8,128)(2,1)S(1)}, u32[]{:S(2)}, u32[]{:S(2)}) %collective-permute-start.11) | collective-permute-done | bytes 393248 | tf_op jit(solution)/shard_map/ppermute | solution.py:22
  77.3 4.0 %collective-permute-start.33 = (bf16[128,512]{1,0:T(8,128)(2,1)S(1)}, bf16[128,512]{1,0:T(8,128)(2,1)S(1)}, u32[]{:S(2)}, u32[]{:S(2)}) collective-permute-start(bf16[128,512]{1,0:T(8,128)(2,1)S(1)} %get-tuple-element.132), channel_id=1, source_target_pairs={{0,24},{4,28},{8,16},{12,20},{16,8},{20,12},{24,0},{28,4},{1,25},{... | collective-permute-start | bytes 393224 | tf_op jit(solution)/shard_map/ppermute | solution.py:22
  81.3 2.0 %collective-permute-start.13 = (bf16[128,512]{1,0:T(8,128)(2,1)S(1)}, bf16[128,512]{1,0:T(8,128)(2,1)S(1)}, u32[]{:S(2)}, u32[]{:S(2)}) collective-permute-start(bf16[128,512]{1,0:T(8,128)(2,1)S(1)} %get-tuple-element.129), channel_id=1, source_target_pairs={{0,8},{4,12},{8,0},{12,4},{16,24},{20,28},{24,16},{28,20},{1,9},{5... | collective-permute-start | bytes 393224 | tf_op jit(solution)/shard_map/ppermute | solution.py:22
  85.4 2.8 %collective-permute-done.33.refs_6_ = bf16[128,512]{1,0:T(8,128)(2,1)S(1)} collective-permute-done((bf16[128,512]{1,0:T(8,128)(2,1)S(1)}, bf16[128,512]{1,0:T(8,128)(2,1)S(1)}, u32[]{:S(2)}, u32[]{:S(2)}) %collective-permute-start.33) | collective-permute-done | bytes 131104 | tf_op jit(solution)/shard_map/ppermute | solution.py:22
  93.2 7.0 %collective-permute-done.36.refs_2_ = bf16[256,512]{1,0:T(8,128)(2,1)S(1)} collective-permute-done((bf16[256,512]{1,0:T(8,128)(2,1)S(1)}, bf16[256,512]{1,0:T(8,128)(2,1)S(1)}, u32[]{:S(2)}, u32[]{:S(2)}) %collective-permute-start.36) | collective-permute-done | bytes 262176 | tf_op jit(solution)/shard_map/ppermute | solution.py:22
  103.4 3.7 %shard_map.197 = (bf16[2048,256]{1,0:T(8,128)(2,1)}, bf16[2048,256]{1,0:T(8,128)(2,1)}) custom-call(bf16[1024,2048]{1,0:T(8,128)(2,1)S(1)} %bitcast.11, bf16[128,256]{1,0:T(8,128)(2,1)S(1)} %get-tuple-element.105.refs_0_, bf16[128,256]{1,0:T(8,128)(2,1)S(1)} %get-tuple-element.106.refs_1_, bf16[384,256]{1,0:T(8,128)(2,1)S(1)} %get-tuple-element.107.refs_2_, ...), custom_call_target="tpu_custom_call" | custom-call | flops 2147483648 | bytes 7340032 | tf_op jit(solution)/shard_map/pallas_call | solution.py:267
  108.6 2.7 %collective-permute-start.38 = (bf16[256,128]{1,0:T(8,128)(2,1)S(1)}, bf16[256,128]{1,0:T(8,128)(2,1)S(1)}, u32[]{:S(2)}, u32[]{:S(2)}) collective-permute-start(bf16[256,128]{1,0:T(8,128)(2,1)S(1)} %get-tuple-element.119), channel_id=1, source_target_pairs={{0,4},{4,0},{8,12},{12,8},{16,20},{20,16},{24,28},{28,24},{1,5},{5... | collective-permute-start | bytes 196616 | tf_op jit(solution)/shard_map/ppermute | solution.py:22
  115.3 3.4 %collective-permute-start.43 = (bf16[256,128]{1,0:T(8,128)(2,1)S(1)}, bf16[256,128]{1,0:T(8,128)(2,1)S(1)}, u32[]{:S(2)}, u32[]{:S(2)}) collective-permute-start(bf16[256,128]{1,0:T(8,128)(2,1)S(1)} %get-tuple-element.136), channel_id=1, source_target_pairs={{0,24},{4,28},{8,16},{12,20},{16,8},{20,12},{24,0},{28,4},{1,25},{... | collective-permute-start | bytes 196616 | tf_op jit(solution)/shard_map/ppermute | solution.py:22
  118.7 2.5 %shard_map.198 = bf16[256,2048]{1,0:T(8,128)(2,1)} custom-call(bf16[512,256]{1,0:T(8,128)(2,1)S(1)} %get-tuple-element.115.refs_0_, bf16[512,256]{1,0:T(8,128)(2,1)S(1)} %get-tuple-element.116.refs_1_, bf16[128,512]{1,0:T(8,128)(2,1)S(1)} %get-tuple-element.75.refs_0_.refs_2_, bf16[128,512]{1,0:T(8,128)(2,1)S(1)} %get-tuple-element.76.refs_1_.refs_3_, ...), custom_call_target="tpu_custom_call" | custom-call | flops 1073741824 | bytes 5767168 | tf_op jit(solution)/shard_map/pallas_call | solution.py:267
  (115 shorter events, 40.5 us)
Async XLA Ops:
  2.2 14.1 %collective-permute-start.15 = (bf16[128,512]{1,0:T(8,128)(2,1)S(1)}, bf16[128,512]{1,0:T(8,128)(2,1)S(1)}, u32[]{:S(2)}, u32[]{:S(2)}) collective-permute-start(bf16[128,512]{1,0:T(8,128)(2,1)S(1)} %get-tuple-element.92), channel_id=1, source_target_pairs={{0,16},{4,20},{8,24},{12,28},{16,0},{20,4},{24,8},{28,12},{1,17},{... | collective-permute-start | bytes 393224 | tf_op jit(solution)/shard_map/ppermute | solution.py:22
  6.3 12.9 %collective-permute-start.16 = (bf16[128,512]{1,0:T(8,128)(2,1)S(1)}, bf16[128,512]{1,0:T(8,128)(2,1)S(1)}, u32[]{:S(2)}, u32[]{:S(2)}) collective-permute-start(bf16[128,512]{1,0:T(8,128)(2,1)S(1)} %get-tuple-element.93), channel_id=1, source_target_pairs={{0,20},{4,16},{8,28},{12,24},{16,4},{20,0},{24,12},{28,8},{1,21},{... | collective-permute-start | bytes 393224 | tf_op jit(solution)/shard_map/ppermute | solution.py:22
  7.6 15.3 %collective-permute-start.3 = (bf16[128,512]{1,0:T(8,128)(2,1)S(1)}, bf16[128,512]{1,0:T(8,128)(2,1)S(1)}, u32[]{:S(2)}, u32[]{:S(2)}) collective-permute-start(bf16[128,512]{1,0:T(8,128)(2,1)S(1)} %get-tuple-element.83), channel_id=1, source_target_pairs={{0,4},{4,0},{8,12},{12,8},{16,20},{20,16},{24,28},{28,24},{1,5},{5... | collective-permute-start | bytes 393224 | tf_op jit(solution)/shard_map/ppermute | solution.py:22
  7.9 16.6 %collective-permute-start.4 = (bf16[128,512]{1,0:T(8,128)(2,1)S(1)}, bf16[128,512]{1,0:T(8,128)(2,1)S(1)}, u32[]{:S(2)}, u32[]{:S(2)}) collective-permute-start(bf16[128,512]{1,0:T(8,128)(2,1)S(1)} %get-tuple-element.84), channel_id=1, source_target_pairs={{0,8},{4,12},{8,0},{12,4},{16,24},{20,28},{24,16},{28,20},{1,9},{5... | collective-permute-start | bytes 393224 | tf_op jit(solution)/shard_map/ppermute | solution.py:22
  9.7 14.9 %collective-permute-start.5 = (bf16[128,512]{1,0:T(8,128)(2,1)S(1)}, bf16[128,512]{1,0:T(8,128)(2,1)S(1)}, u32[]{:S(2)}, u32[]{:S(2)}) collective-permute-start(bf16[128,512]{1,0:T(8,128)(2,1)S(1)} %get-tuple-element.85), channel_id=1, source_target_pairs={{0,12},{4,8},{8,4},{12,0},{16,28},{20,24},{24,20},{28,16},{1,13},{... | collective-permute-start | bytes 393224 | tf_op jit(solution)/shard_map/ppermute | solution.py:22
  22.9 9.2 %collective-permute-start.18 = (bf16[256,512]{1,0:T(8,128)(2,1)S(1)}, bf16[256,512]{1,0:T(8,128)(2,1)S(1)}, u32[]{:S(2)}, u32[]{:S(2)}) collective-permute-start(bf16[256,512]{1,0:T(8,128)(2,1)S(1)} %constant_dynamic-update-slice_fusion.3.refs_0_.refs_10_), channel_id=1, source_target_pairs={{0,2},{1,3},{2,0},{3,1},{4,6},{5,7},{6,4},{7,5},{8,10},{9,11},{10,... | collective-permute-start | bytes 786440 | tf_op jit(solution)/shard_map/ppermute | solution.py:22
  24.5 20.4 %collective-permute-start.17 = (bf16[256,512]{1,0:T(8,128)(2,1)S(1)}, bf16[256,512]{1,0:T(8,128)(2,1)S(1)}, u32[]{:S(2)}, u32[]{:S(2)}) collective-permute-start(bf16[256,512]{1,0:T(8,128)(2,1)S(1)} %constant_dynamic-update-slice_fusion.3.refs_0_.refs_10_), channel_id=1, source_target_pairs={{0,1},{1,0},{2,3},{3,2},{4,5},{5,4},{6,7},{7,6},{8,9},{9,8},{10,11... | collective-permute-start | bytes 786440 | tf_op jit(solution)/shard_map/ppermute | solution.py:22
  24.6 20.7 %collective-permute-start.7 = (bf16[384,512]{1,0:T(8,128)(2,1)S(1)}, bf16[384,512]{1,0:T(8,128)(2,1)S(1)}, u32[]{:S(2)}, u32[]{:S(2)}) collective-permute-start(bf16[384,512]{1,0:T(8,128)(2,1)S(1)} %constant_dynamic-update-slice_fusion.refs_0_.refs_6_), channel_id=1, source_target_pairs={{0,2},{1,3},{2,0},{3,1},{4,6},{5,7},{6,4},{7,5},{8,10},{9,11},{10,... | collective-permute-start | bytes 1179656 | tf_op jit(solution)/shard_map/ppermute | solution.py:22
  27.2 17.6 %collective-permute-start.28 = (bf16[256,512]{1,0:T(8,128)(2,1)S(1)}, bf16[256,512]{1,0:T(8,128)(2,1)S(1)}, u32[]{:S(2)}, u32[]{:S(2)}) collective-permute-start(bf16[256,512]{1,0:T(8,128)(2,1)S(1)} %constant_dynamic-update-slice_fusion.5.refs_0_.refs_14_), channel_id=1, source_target_pairs={{0,2},{1,3},{2,0},{3,1},{4,6},{5,7},{6,4},{7,5},{8,10},{9,11},{10,... | collective-permute-start | bytes 786440 | tf_op jit(solution)/shard_map/ppermute | solution.py:22
  32.1 13.3 %collective-permute-start.19 = (bf16[256,512]{1,0:T(8,128)(2,1)S(1)}, bf16[256,512]{1,0:T(8,128)(2,1)S(1)}, u32[]{:S(2)}, u32[]{:S(2)}) collective-permute-start(bf16[256,512]{1,0:T(8,128)(2,1)S(1)} %collective-permute-done.18.refs_2_.refs_12_), channel_id=1, source_target_pairs={{0,1},{1,0},{2,3},{3,2},{4,5},{5,4},{6,7},{7,6},{8,9},{9,8},{10,11... | collective-permute-start | bytes 786440 | tf_op jit(solution)/shard_map/ppermute | solution.py:22
  47.7 29.6 %collective-permute-start = (bf16[128,512]{1,0:T(8,128)(2,1)S(1)}, bf16[128,512]{1,0:T(8,128)(2,1)S(1)}, u32[]{:S(2)}, u32[]{:S(2)}) collective-permute-start(bf16[128,512]{1,0:T(8,128)(2,1)S(1)} %get-tuple-element.80), channel_id=1, source_target_pairs={{0,1},{1,0},{2,3},{3,2},{4,5},{5,4},{6,7},{7,6},{8,9},{9,8},{10,11... | collective-permute-start | bytes 393224 | tf_op jit(solution)/shard_map/ppermute | solution.py:22
  48.2 33.1 %collective-permute-start.2 = (bf16[128,512]{1,0:T(8,128)(2,1)S(1)}, bf16[128,512]{1,0:T(8,128)(2,1)S(1)}, u32[]{:S(2)}, u32[]{:S(2)}) collective-permute-start(bf16[128,512]{1,0:T(8,128)(2,1)S(1)} %add_convert_fusion.8), channel_id=1, source_target_pairs={{0,2},{1,3},{2,0},{3,1},{4,6},{5,7},{6,4},{7,5},{8,10},{9,11},{10,... | collective-permute-start | bytes 393224 | tf_op jit(solution)/shard_map/ppermute | solution.py:22
  52.1 9.2 %collective-permute-start.22 = (bf16[256,512]{1,0:T(8,128)(2,1)S(1)}, bf16[256,512]{1,0:T(8,128)(2,1)S(1)}, u32[]{:S(2)}, u32[]{:S(2)}) collective-permute-start(bf16[256,512]{1,0:T(8,128)(2,1)S(1)} %add_convert_fusion.5), channel_id=1, source_target_pairs={{0,2},{1,3},{2,0},{3,1},{4,6},{5,7},{6,4},{7,5},{8,10},{9,11},{10,... | collective-permute-start | bytes 786440 | tf_op jit(solution)/shard_map/ppermute | solution.py:22
  55.0 11.0 %collective-permute-start.32 = (bf16[256,512]{1,0:T(8,128)(2,1)S(1)}, bf16[256,512]{1,0:T(8,128)(2,1)S(1)}, u32[]{:S(2)}, u32[]{:S(2)}) collective-permute-start(bf16[256,512]{1,0:T(8,128)(2,1)S(1)} %add_convert_fusion.3), channel_id=1, source_target_pairs={{0,2},{1,3},{2,0},{3,1},{4,6},{5,7},{6,4},{7,5},{8,10},{9,11},{10,... | collective-permute-start | bytes 786440 | tf_op jit(solution)/shard_map/ppermute | solution.py:22
  63.2 18.0 %collective-permute-start.24 = (bf16[128,512]{1,0:T(8,128)(2,1)S(1)}, bf16[128,512]{1,0:T(8,128)(2,1)S(1)}, u32[]{:S(2)}, u32[]{:S(2)}) collective-permute-start(bf16[128,512]{1,0:T(8,128)(2,1)S(1)} %get-tuple-element.133), channel_id=1, source_target_pairs={{0,20},{4,16},{8,28},{12,24},{16,4},{20,0},{24,12},{28,8},{1,21},{... | collective-permute-start | bytes 393224 | tf_op jit(solution)/shard_map/ppermute | solution.py:22
  66.0 10.2 %collective-permute-start.11 = (bf16[384,512]{1,0:T(8,128)(2,1)S(1)}, bf16[384,512]{1,0:T(8,128)(2,1)S(1)}, u32[]{:S(2)}, u32[]{:S(2)}) collective-permute-start(bf16[384,512]{1,0:T(8,128)(2,1)S(1)} %add_convert_fusion.1), channel_id=1, source_target_pairs={{0,2},{1,3},{2,0},{3,1},{4,6},{5,7},{6,4},{7,5},{8,10},{9,11},{10,... | collective-permute-start | bytes 1179656 | tf_op jit(solution)/shard_map/ppermute | solution.py:22
  66.6 16.6 %collective-permute-start.23 = (bf16[128,512]{1,0:T(8,128)(2,1)S(1)}, bf16[128,512]{1,0:T(8,128)(2,1)S(1)}, u32[]{:S(2)}, u32[]{:S(2)}) collective-permute-start(bf16[128,512]{1,0:T(8,128)(2,1)S(1)} %get-tuple-element.134), channel_id=1, source_target_pairs={{0,16},{4,20},{8,24},{12,28},{16,0},{20,4},{24,8},{28,12},{1,17},{... | collective-permute-start | bytes 393224 | tf_op jit(solution)/shard_map/ppermute | solution.py:22
  76.2 9.1 %collective-permute-start.34 = (bf16[128,512]{1,0:T(8,128)(2,1)S(1)}, bf16[128,512]{1,0:T(8,128)(2,1)S(1)}, u32[]{:S(2)}, u32[]{:S(2)}) collective-permute-start(bf16[128,512]{1,0:T(8,128)(2,1)S(1)} %get-tuple-element.131), channel_id=1, source_target_pairs={{0,28},{4,24},{8,20},{12,16},{16,12},{20,8},{24,4},{28,0},{1,29},{... | collective-permute-start | bytes 393224 | tf_op jit(solution)/shard_map/ppermute | solution.py:22
  77.3 10.9 %collective-permute-start.33 = (bf16[128,512]{1,0:T(8,128)(2,1)S(1)}, bf16[128,512]{1,0:T(8,128)(2,1)S(1)}, u32[]{:S(2)}, u32[]{:S(2)}) collective-permute-start(bf16[128,512]{1,0:T(8,128)(2,1)S(1)} %get-tuple-element.132), channel_id=1, source_target_pairs={{0,24},{4,28},{8,16},{12,20},{16,8},{20,12},{24,0},{28,4},{1,25},{... | collective-permute-start | bytes 393224 | tf_op jit(solution)/shard_map/ppermute | solution.py:22
  81.3 10.0 %collective-permute-start.13 = (bf16[128,512]{1,0:T(8,128)(2,1)S(1)}, bf16[128,512]{1,0:T(8,128)(2,1)S(1)}, u32[]{:S(2)}, u32[]{:S(2)}) collective-permute-start(bf16[128,512]{1,0:T(8,128)(2,1)S(1)} %get-tuple-element.129), channel_id=1, source_target_pairs={{0,8},{4,12},{8,0},{12,4},{16,24},{20,28},{24,16},{28,20},{1,9},{5... | collective-permute-start | bytes 393224 | tf_op jit(solution)/shard_map/ppermute | solution.py:22
  103.4 10.8 %collective-permute-start.41 = (bf16[512,128]{1,0:T(8,128)(2,1)S(1)}, bf16[512,128]{1,0:T(8,128)(2,1)S(1)}, u32[]{:S(2)}, u32[]{:S(2)}) collective-permute-start(bf16[512,128]{1,0:T(8,128)(2,1)S(1)} %get-tuple-element.123), channel_id=1, source_target_pairs={{0,4},{4,0},{8,12},{12,8},{16,20},{20,16},{24,28},{28,24},{1,5},{5... | collective-permute-start | bytes 393224 | tf_op jit(solution)/shard_map/ppermute | solution.py:22
  108.6 13.3 %collective-permute-start.38 = (bf16[256,128]{1,0:T(8,128)(2,1)S(1)}, bf16[256,128]{1,0:T(8,128)(2,1)S(1)}, u32[]{:S(2)}, u32[]{:S(2)}) collective-permute-start(bf16[256,128]{1,0:T(8,128)(2,1)S(1)} %get-tuple-element.119), channel_id=1, source_target_pairs={{0,4},{4,0},{8,12},{12,8},{16,20},{20,16},{24,28},{28,24},{1,5},{5... | collective-permute-start | bytes 196616 | tf_op jit(solution)/shard_map/ppermute | solution.py:22
  111.3 10.6 %collective-permute-start.39 = (bf16[256,128]{1,0:T(8,128)(2,1)S(1)}, bf16[256,128]{1,0:T(8,128)(2,1)S(1)}, u32[]{:S(2)}, u32[]{:S(2)}) collective-permute-start(bf16[256,128]{1,0:T(8,128)(2,1)S(1)} %get-tuple-element.120), channel_id=1, source_target_pairs={{0,8},{4,12},{8,0},{12,4},{16,24},{20,28},{24,16},{28,20},{1,9},{5... | collective-permute-start | bytes 196616 | tf_op jit(solution)/shard_map/ppermute | solution.py:22
  112.8 9.2 %collective-permute-start.40 = (bf16[256,128]{1,0:T(8,128)(2,1)S(1)}, bf16[256,128]{1,0:T(8,128)(2,1)S(1)}, u32[]{:S(2)}, u32[]{:S(2)}) collective-permute-start(bf16[256,128]{1,0:T(8,128)(2,1)S(1)} %get-tuple-element.121), channel_id=1, source_target_pairs={{0,12},{4,8},{8,4},{12,0},{16,28},{20,24},{24,20},{28,16},{1,13},{... | collective-permute-start | bytes 196616 | tf_op jit(solution)/shard_map/ppermute | solution.py:22
  (28 other events, 327.7 us)

commit v3 on v2

--- a/solution.py
+++ b/solution.py
@@ -214,16 +214,14 @@
         out[...] = total.astype(BF16)
 
 
-def combine_kernel(select, cot, *refs):
-    blocks, (out, kept) = refs[:-2], refs[-2:]
-    total = cot[...].astype(F32)
-    start = 0
-    for block in blocks:
+def combine_kernel(starts, select, base, *refs):
+    blocks, outs = refs[: len(starts)], refs[len(starts) :]
+    total = base[...].astype(F32)
+    for start, block in zip(starts, blocks):
         size = block.shape[0]
         total = total + dot(select[:, start : start + size], block[...], ((1,), (0,)))
-        start += size
-    out[...] = total.astype(BF16)
-    kept[...] = total.astype(BF16)
+    for out in outs:
+        out[...] = total.astype(out.dtype)
 
 
 def mixer_kernel(lanes, direct, gate_in, conv_sum, w_out, *refs):
@@ -447,9 +445,20 @@
         4 * slots * model_width * units,
         28,
     )
+    soon = [k for k in (0, 4, 5) if k in returned] if direct else []
+    late = [k for k in sorted(returned) if k not in soon]
+    base = own_cot
+    if soon:
+        (base,) = flat_call(
+            functools.partial(combine_kernel, [k * capacity for k in soon]),
+            (select, own_cot, *[returned[k] for k in soon]),
+            [struct((tokens, cols), F32)],
+            2 * len(soon) * capacity * tokens * cols,
+            16,
+        )
     grad_input, kept = flat_call(
-        combine_kernel,
-        (select, own_cot, *[returned[k] for k in sorted(returned)]),
+        functools.partial(combine_kernel, [k * capacity for k in late]),
+        (select, base, *[returned[k] for k in late]),
         [struct((tokens, cols), BF16)] * 2,
         2 * slots * tokens * cols,
         16,

time: 123 us -> 123 us (level)
    pallas_call x13 -> x14, Pallas kernels: 26.7 us -> 26.9 us  [flat_call(): pl.pallas_call(kernel, in_specs=[pl.BlockSpec(memory_space=space[i] if is...]
where the time goes in v3:
time: 123 us; the launch traced here: 122 us
  starting transfers between devices  48 us (39%)
  waiting for transfers between devices  45 us (37%)
  Pallas kernels  26.9 us (22%)
  other arithmetic  1.41 us (1%)
    ppermute x44, starting transfers between devices, swap(): return lax.ppermute(value, axis, route)  46.6 us
    ppermute x44, waiting for transfers between devices, swap(): return lax.ppermute(value, axis, route)  45 us
    pallas_call x14, Pallas kernels, flat_call(): pl.pallas_call(kernel, in_specs=[pl.BlockSpec(memory_space=space[i] if is...  26.9 us
  transfers between devices with their start and end apart: 45, of which 15 were waited for; matrix products, arithmetic and copies ran while one was open for 1% of the time, Pallas kernels for 18%

profile of v3, /device:TPU:0, one launch (start us, length us, event | category | flops | bytes accessed | tf_op | source)
XLA Modules:
  0.0 122.5 jit_solution(10477710896693199423)
XLA Ops:
  2.2 4.1 %collective-permute-start.3 = (bf16[128,512]{1,0:T(8,128)(2,1)S(1)}, bf16[128,512]{1,0:T(8,128)(2,1)S(1)}, u32[]{:S(2)}, u32[]{:S(2)}) collective-permute-start(bf16[128,512]{1,0:T(8,128)(2,1)S(1)} %get-tuple-element.85), channel_id=1, source_target_pairs={{0,16},{4,20},{8,24},{12,28},{16,0},{20,4},{24,8},{28,12},{1,17},{... | collective-permute-start | bytes 393224 | tf_op jit(solution)/shard_map/ppermute | solution.py:22
  7.9 1.8 %collective-permute-start.14 = (bf16[128,512]{1,0:T(8,128)(2,1)S(1)}, bf16[128,512]{1,0:T(8,128)(2,1)S(1)}, u32[]{:S(2)}, u32[]{:S(2)}) collective-permute-start(bf16[128,512]{1,0:T(8,128)(2,1)S(1)} %get-tuple-element.92), channel_id=1, source_target_pairs={{0,8},{4,12},{8,0},{12,4},{16,24},{20,28},{24,16},{28,20},{1,9},{5... | collective-permute-start | bytes 393224 | tf_op jit(solution)/shard_map/ppermute | solution.py:22
  11.1 5.2 %collective-permute-done.3 = bf16[128,512]{1,0:T(8,128)(2,1)S(1)} collective-permute-done((bf16[128,512]{1,0:T(8,128)(2,1)S(1)}, bf16[128,512]{1,0:T(8,128)(2,1)S(1)}, u32[]{:S(2)}, u32[]{:S(2)}) %collective-permute-start.3) | collective-permute-done | bytes 131104 | tf_op jit(solution)/shard_map/ppermute | solution.py:22
  16.3 2.9 %collective-permute-start.25 = (bf16[128,512]{1,0:T(8,128)(2,1)S(1)}, bf16[128,512]{1,0:T(8,128)(2,1)S(1)}, u32[]{:S(2)}, u32[]{:S(2)}) collective-permute-start(bf16[128,512]{1,0:T(8,128)(2,1)S(1)} %get-tuple-element.98), channel_id=1, source_target_pairs={{0,24},{4,28},{8,16},{12,20},{16,8},{20,12},{24,0},{28,4},{1,25},{... | collective-permute-start | bytes 393224 | tf_op jit(solution)/shard_map/ppermute | solution.py:22
  19.3 3.6 %collective-permute-start.26 = (bf16[128,512]{1,0:T(8,128)(2,1)S(1)}, bf16[128,512]{1,0:T(8,128)(2,1)S(1)}, u32[]{:S(2)}, u32[]{:S(2)}) collective-permute-start(bf16[128,512]{1,0:T(8,128)(2,1)S(1)} %get-tuple-element.99), channel_id=1, source_target_pairs={{0,28},{4,24},{8,20},{12,16},{16,12},{20,8},{24,4},{28,0},{1,29},{... | collective-permute-start | bytes 393224 | tf_op jit(solution)/shard_map/ppermute | solution.py:22
  25.2 2.0 %collective-permute-done.26 = bf16[128,512]{1,0:T(8,128)(2,1)S(1)} collective-permute-done((bf16[128,512]{1,0:T(8,128)(2,1)S(1)}, bf16[128,512]{1,0:T(8,128)(2,1)S(1)}, u32[]{:S(2)}, u32[]{:S(2)}) %collective-permute-start.26) | collective-permute-done | bytes 131104 | tf_op jit(solution)/shard_map/ppermute | solution.py:22
  28.8 3.3 %collective-permute-done.6.refs_2_.refs_12_ = bf16[256,512]{1,0:T(8,128)(2,1)S(1)} collective-permute-done((bf16[256,512]{1,0:T(8,128)(2,1)S(1)}, bf16[256,512]{1,0:T(8,128)(2,1)S(1)}, u32[]{:S(2)}, u32[]{:S(2)}) %collective-permute-start.6) | collective-permute-done | bytes 262176 | tf_op jit(solution)/shard_map/ppermute | solution.py:22
  32.1 2.3 %shard_map.188 = (bf16[2048,256]{1,0:T(8,128)(2,1)S(1)}, bf16[2048,256]{1,0:T(8,128)(2,1)S(1)}, bf16[256,2048]{1,0:T(8,128)(2,1)S(1)}, bf16[256,1024]{1,0:T(8,12...) custom-call(s32[2,256]{1,0:T(2,128)} %bitcast.17, ...), custom_call_target="tpu_custom_call" | custom-call | flops 268435456 | bytes 8654848 | tf_op jit(solution)/shard_map/pallas_call | solution.py:265
  34.4 2.9 %shard_map.189 = (bf16[512,256]{1,0:T(8,128)(2,1)S(1)}, f32[512,256]{1,0:T(8,128)S(1)}, f32[512,256]{1,0:T(8,128)S(1)}) custom-call(bf16[1024,2048]{1,0:T(8,128)(2,1)} %bitcast.9, bf16[2048,256]{1,0:T(8,128)(2,1)S(1)} %get-tuple-element.70.w_gate, bf16[2048,256]{1,0:T(8,128)(2,1)S(1)} %get-tuple-element.71.w_up), custom_call_target="tpu_custom_call" | custom-call | flops 1073741824 | bytes 7602176 | tf_op jit(solution)/shard_map/pallas_call | solution.py:265
  37.3 1.6 %shard_map.190 = (bf16[128,256]{1,0:T(8,128)(2,1)S(1)}, bf16[128,256]{1,0:T(8,128)(2,1)S(1)}, bf16[128,512]{1,0:T(8,128)(2,1)S(1)}, bf16[128,512]{1,0:T(8,128)(2...) custom-call(f32[512,256]{1,0:T(8,128)S(1)} %get-tuple-element.72.slope, ...), custom_call_target="tpu_custom_call" | custom-call | flops 402653184 | bytes 5373952 | tf_op jit(solution)/shard_map/pallas_call | solution.py:265
  39.5 2.9 %shard_map.191 = (bf16[512,256]{1,0:T(8,128)(2,1)S(1)}, f32[512,256]{1,0:T(8,128)S(1)}, f32[512,256]{1,0:T(8,128)S(1)}) custom-call(bf16[1024,2048]{1,0:T(8,128)(2,1)} %bitcast.10, bf16[2048,256]{1,0:T(8,128)(2,1)S(1)} %get-tuple-element.70.w_gate, bf16[2048,256]{1,0:T(8,128)(2,1)S(1)} %get-tuple-element.71.w_up), custom_call_target="tpu_custom_call" | custom-call | flops 1073741824 | bytes 7602176 | tf_op jit(solution)/shard_map/pallas_call | solution.py:265
  42.5 2.4 %collective-permute-done.28.refs_2_.refs_16_ = bf16[256,512]{1,0:T(8,128)(2,1)S(1)} collective-permute-done((bf16[256,512]{1,0:T(8,128)(2,1)S(1)}, bf16[256,512]{1,0:T(8,128)(2,1)S(1)}, u32[]{:S(2)}, u32[]{:S(2)}) %collective-permute-start.28) | collective-permute-done | bytes 262176 | tf_op jit(solution)/shard_map/ppermute | solution.py:22
  52.6 2.3 %shard_map.195 = (bf16[384,256]{1,0:T(8,128)(2,1)S(1)}, bf16[384,256]{1,0:T(8,128)(2,1)S(1)}, bf16[384,512]{1,0:T(8,128)(2,1)S(1)}, bf16[384,512]{1,0:T(8,128)(2...) custom-call(f32[512,256]{1,0:T(8,128)S(1)} %get-tuple-element.72.slope, ...), custom_call_target="tpu_custom_call" | custom-call | flops 1207959552 | bytes 7733248 | tf_op jit(solution)/shard_map/pallas_call | solution.py:265
  56.6 4.6 %collective-permute-done.10 = bf16[256,512]{1,0:T(8,128)(2,1)S(1)} collective-permute-done((bf16[256,512]{1,0:T(8,128)(2,1)S(1)}, bf16[256,512]{1,0:T(8,128)(2,1)S(1)}, u32[]{:S(2)}, u32[]{:S(2)}) %collective-permute-start.10) | collective-permute-done | bytes 262176 | tf_op jit(solution)/shard_map/ppermute | solution.py:22
  63.3 2.6 %collective-permute-done.32 = bf16[256,512]{1,0:T(8,128)(2,1)S(1)} collective-permute-done((bf16[256,512]{1,0:T(8,128)(2,1)S(1)}, bf16[256,512]{1,0:T(8,128)(2,1)S(1)}, u32[]{:S(2)}, u32[]{:S(2)}) %collective-permute-start.32) | collective-permute-done | bytes 262176 | tf_op jit(solution)/shard_map/ppermute | solution.py:22
  67.9 8.3 %collective-permute-done.21 = bf16[384,512]{1,0:T(8,128)(2,1)S(1)} collective-permute-done((bf16[384,512]{1,0:T(8,128)(2,1)S(1)}, bf16[384,512]{1,0:T(8,128)(2,1)S(1)}, u32[]{:S(2)}, u32[]{:S(2)}) %collective-permute-start.21) | collective-permute-done | bytes 393248 | tf_op jit(solution)/shard_map/ppermute | solution.py:22
  77.3 4.0 %collective-permute-start.33 = (bf16[128,512]{1,0:T(8,128)(2,1)S(1)}, bf16[128,512]{1,0:T(8,128)(2,1)S(1)}, u32[]{:S(2)}, u32[]{:S(2)}) collective-permute-start(bf16[128,512]{1,0:T(8,128)(2,1)S(1)} %get-tuple-element.132), channel_id=1, source_target_pairs={{0,24},{4,28},{8,16},{12,20},{16,8},{20,12},{24,0},{28,4},{1,25},{... | collective-permute-start | bytes 393224 | tf_op jit(solution)/shard_map/ppermute | solution.py:22
  81.3 2.0 %collective-permute-start.23 = (bf16[128,512]{1,0:T(8,128)(2,1)S(1)}, bf16[128,512]{1,0:T(8,128)(2,1)S(1)}, u32[]{:S(2)}, u32[]{:S(2)}) collective-permute-start(bf16[128,512]{1,0:T(8,128)(2,1)S(1)} %get-tuple-element.129), channel_id=1, source_target_pairs={{0,8},{4,12},{8,0},{12,4},{16,24},{20,28},{24,16},{28,20},{1,9},{5... | collective-permute-start | bytes 393224 | tf_op jit(solution)/shard_map/ppermute | solution.py:22
  85.4 2.8 %collective-permute-done.33.refs_3_ = bf16[128,512]{1,0:T(8,128)(2,1)S(1)} collective-permute-done((bf16[128,512]{1,0:T(8,128)(2,1)S(1)}, bf16[128,512]{1,0:T(8,128)(2,1)S(1)}, u32[]{:S(2)}, u32[]{:S(2)}) %collective-permute-start.33) | collective-permute-done | bytes 131104 | tf_op jit(solution)/shard_map/ppermute | solution.py:22
  93.0 7.0 %collective-permute-done.36.refs_2_ = bf16[256,512]{1,0:T(8,128)(2,1)S(1)} collective-permute-done((bf16[256,512]{1,0:T(8,128)(2,1)S(1)}, bf16[256,512]{1,0:T(8,128)(2,1)S(1)}, u32[]{:S(2)}, u32[]{:S(2)}) %collective-permute-start.36) | collective-permute-done | bytes 262176 | tf_op jit(solution)/shard_map/ppermute | solution.py:22
  103.2 3.7 %shard_map.198 = (bf16[2048,256]{1,0:T(8,128)(2,1)}, bf16[2048,256]{1,0:T(8,128)(2,1)}) custom-call(bf16[1024,2048]{1,0:T(8,128)(2,1)S(1)} %bitcast.11, bf16[128,256]{1,0:T(8,128)(2,1)S(1)} %get-tuple-element.105.refs_0_, bf16[128,256]{1,0:T(8,128)(2,1)S(1)} %get-tuple-element.106.refs_1_, bf16[384,256]{1,0:T(8,128)(2,1)S(1)} %get-tuple-element.107.refs_2_, ...), custom_call_target="tpu_custom_call" | custom-call | flops 2147483648 | bytes 7340032 | tf_op jit(solution)/shard_map/pallas_call | solution.py:265
  108.4 2.7 %collective-permute-start.38 = (bf16[256,128]{1,0:T(8,128)(2,1)S(1)}, bf16[256,128]{1,0:T(8,128)(2,1)S(1)}, u32[]{:S(2)}, u32[]{:S(2)}) collective-permute-start(bf16[256,128]{1,0:T(8,128)(2,1)S(1)} %get-tuple-element.119), channel_id=1, source_target_pairs={{0,4},{4,0},{8,12},{12,8},{16,20},{20,16},{24,28},{28,24},{1,5},{5... | collective-permute-start | bytes 196616 | tf_op jit(solution)/shard_map/ppermute | solution.py:22
  115.1 3.4 %collective-permute-start.43 = (bf16[256,128]{1,0:T(8,128)(2,1)S(1)}, bf16[256,128]{1,0:T(8,128)(2,1)S(1)}, u32[]{:S(2)}, u32[]{:S(2)}) collective-permute-start(bf16[256,128]{1,0:T(8,128)(2,1)S(1)} %get-tuple-element.136), channel_id=1, source_target_pairs={{0,24},{4,28},{8,16},{12,20},{16,8},{20,12},{24,0},{28,4},{1,25},{... | collective-permute-start | bytes 196616 | tf_op jit(solution)/shard_map/ppermute | solution.py:22
  118.5 2.5 %shard_map.199 = bf16[256,2048]{1,0:T(8,128)(2,1)} custom-call(bf16[512,256]{1,0:T(8,128)(2,1)S(1)} %get-tuple-element.115.refs_0_, bf16[512,256]{1,0:T(8,128)(2,1)S(1)} %get-tuple-element.116.refs_1_, bf16[128,512]{1,0:T(8,128)(2,1)S(1)} %get-tuple-element.75.refs_0_.refs_2_, bf16[128,512]{1,0:T(8,128)(2,1)S(1)} %get-tuple-element.76.refs_1_.refs_3_, ...), custom_call_target="tpu_custom_call" | custom-call | flops 1073741824 | bytes 5767168 | tf_op jit(solution)/shard_map/pallas_call | solution.py:265
  (116 shorter events, 40.4 us)
Async XLA Ops:
  2.2 14.1 %collective-permute-start.3 = (bf16[128,512]{1,0:T(8,128)(2,1)S(1)}, bf16[128,512]{1,0:T(8,128)(2,1)S(1)}, u32[]{:S(2)}, u32[]{:S(2)}) collective-permute-start(bf16[128,512]{1,0:T(8,128)(2,1)S(1)} %get-tuple-element.85), channel_id=1, source_target_pairs={{0,16},{4,20},{8,24},{12,28},{16,0},{20,4},{24,8},{28,12},{1,17},{... | collective-permute-start | bytes 393224 | tf_op jit(solution)/shard_map/ppermute | solution.py:22
  6.3 12.9 %collective-permute-start.4 = (bf16[128,512]{1,0:T(8,128)(2,1)S(1)}, bf16[128,512]{1,0:T(8,128)(2,1)S(1)}, u32[]{:S(2)}, u32[]{:S(2)}) collective-permute-start(bf16[128,512]{1,0:T(8,128)(2,1)S(1)} %get-tuple-element.86), channel_id=1, source_target_pairs={{0,20},{4,16},{8,28},{12,24},{16,4},{20,0},{24,12},{28,8},{1,21},{... | collective-permute-start | bytes 393224 | tf_op jit(solution)/shard_map/ppermute | solution.py:22
  7.6 15.3 %collective-permute-start.13 = (bf16[128,512]{1,0:T(8,128)(2,1)S(1)}, bf16[128,512]{1,0:T(8,128)(2,1)S(1)}, u32[]{:S(2)}, u32[]{:S(2)}) collective-permute-start(bf16[128,512]{1,0:T(8,128)(2,1)S(1)} %get-tuple-element.91), channel_id=1, source_target_pairs={{0,4},{4,0},{8,12},{12,8},{16,20},{20,16},{24,28},{28,24},{1,5},{5... | collective-permute-start | bytes 393224 | tf_op jit(solution)/shard_map/ppermute | solution.py:22
  7.9 16.6 %collective-permute-start.14 = (bf16[128,512]{1,0:T(8,128)(2,1)S(1)}, bf16[128,512]{1,0:T(8,128)(2,1)S(1)}, u32[]{:S(2)}, u32[]{:S(2)}) collective-permute-start(bf16[128,512]{1,0:T(8,128)(2,1)S(1)} %get-tuple-element.92), channel_id=1, source_target_pairs={{0,8},{4,12},{8,0},{12,4},{16,24},{20,28},{24,16},{28,20},{1,9},{5... | collective-permute-start | bytes 393224 | tf_op jit(solution)/shard_map/ppermute | solution.py:22
  9.7 14.9 %collective-permute-start.15 = (bf16[128,512]{1,0:T(8,128)(2,1)S(1)}, bf16[128,512]{1,0:T(8,128)(2,1)S(1)}, u32[]{:S(2)}, u32[]{:S(2)}) collective-permute-start(bf16[128,512]{1,0:T(8,128)(2,1)S(1)} %get-tuple-element.93), channel_id=1, source_target_pairs={{0,12},{4,8},{8,4},{12,0},{16,28},{20,24},{24,20},{28,16},{1,13},{... | collective-permute-start | bytes 393224 | tf_op jit(solution)/shard_map/ppermute | solution.py:22
  22.9 9.2 %collective-permute-start.6 = (bf16[256,512]{1,0:T(8,128)(2,1)S(1)}, bf16[256,512]{1,0:T(8,128)(2,1)S(1)}, u32[]{:S(2)}, u32[]{:S(2)}) collective-permute-start(bf16[256,512]{1,0:T(8,128)(2,1)S(1)} %constant_dynamic-update-slice_fusion.refs_0_.refs_10_), channel_id=1, source_target_pairs={{0,2},{1,3},{2,0},{3,1},{4,6},{5,7},{6,4},{7,5},{8,10},{9,11},{10,... | collective-permute-start | bytes 786440 | tf_op jit(solution)/shard_map/ppermute | solution.py:22
  24.5 20.4 %collective-permute-start.5 = (bf16[256,512]{1,0:T(8,128)(2,1)S(1)}, bf16[256,512]{1,0:T(8,128)(2,1)S(1)}, u32[]{:S(2)}, u32[]{:S(2)}) collective-permute-start(bf16[256,512]{1,0:T(8,128)(2,1)S(1)} %constant_dynamic-update-slice_fusion.refs_0_.refs_10_), channel_id=1, source_target_pairs={{0,1},{1,0},{2,3},{3,2},{4,5},{5,4},{6,7},{7,6},{8,9},{9,8},{10,11... | collective-permute-start | bytes 786440 | tf_op jit(solution)/shard_map/ppermute | solution.py:22
  24.6 20.7 %collective-permute-start.17 = (bf16[384,512]{1,0:T(8,128)(2,1)S(1)}, bf16[384,512]{1,0:T(8,128)(2,1)S(1)}, u32[]{:S(2)}, u32[]{:S(2)}) collective-permute-start(bf16[384,512]{1,0:T(8,128)(2,1)S(1)} %constant_dynamic-update-slice_fusion.2.refs_0_.refs_6_), channel_id=1, source_target_pairs={{0,2},{1,3},{2,0},{3,1},{4,6},{5,7},{6,4},{7,5},{8,10},{9,11},{10,... | collective-permute-start | bytes 1179656 | tf_op jit(solution)/shard_map/ppermute | solution.py:22
  27.2 17.6 %collective-permute-start.28 = (bf16[256,512]{1,0:T(8,128)(2,1)S(1)}, bf16[256,512]{1,0:T(8,128)(2,1)S(1)}, u32[]{:S(2)}, u32[]{:S(2)}) collective-permute-start(bf16[256,512]{1,0:T(8,128)(2,1)S(1)} %constant_dynamic-update-slice_fusion.5.refs_0_.refs_14_), channel_id=1, source_target_pairs={{0,2},{1,3},{2,0},{3,1},{4,6},{5,7},{6,4},{7,5},{8,10},{9,11},{10,... | collective-permute-start | bytes 786440 | tf_op jit(solution)/shard_map/ppermute | solution.py:22
  32.1 13.3 %collective-permute-start.7 = (bf16[256,512]{1,0:T(8,128)(2,1)S(1)}, bf16[256,512]{1,0:T(8,128)(2,1)S(1)}, u32[]{:S(2)}, u32[]{:S(2)}) collective-permute-start(bf16[256,512]{1,0:T(8,128)(2,1)S(1)} %collective-permute-done.6.refs_2_.refs_12_), channel_id=1, source_target_pairs={{0,1},{1,0},{2,3},{3,2},{4,5},{5,4},{6,7},{7,6},{8,9},{9,8},{10,11... | collective-permute-start | bytes 786440 | tf_op jit(solution)/shard_map/ppermute | solution.py:22
  47.7 29.6 %collective-permute-start = (bf16[128,512]{1,0:T(8,128)(2,1)S(1)}, bf16[128,512]{1,0:T(8,128)(2,1)S(1)}, u32[]{:S(2)}, u32[]{:S(2)}) collective-permute-start(bf16[128,512]{1,0:T(8,128)(2,1)S(1)} %get-tuple-element.80), channel_id=1, source_target_pairs={{0,1},{1,0},{2,3},{3,2},{4,5},{5,4},{6,7},{7,6},{8,9},{9,8},{10,11... | collective-permute-start | bytes 393224 | tf_op jit(solution)/shard_map/ppermute | solution.py:22
  48.2 33.1 %collective-permute-start.2 = (bf16[128,512]{1,0:T(8,128)(2,1)S(1)}, bf16[128,512]{1,0:T(8,128)(2,1)S(1)}, u32[]{:S(2)}, u32[]{:S(2)}) collective-permute-start(bf16[128,512]{1,0:T(8,128)(2,1)S(1)} %add_convert_fusion.8), channel_id=1, source_target_pairs={{0,2},{1,3},{2,0},{3,1},{4,6},{5,7},{6,4},{7,5},{8,10},{9,11},{10,... | collective-permute-start | bytes 393224 | tf_op jit(solution)/shard_map/ppermute | solution.py:22
  52.1 9.2 %collective-permute-start.10 = (bf16[256,512]{1,0:T(8,128)(2,1)S(1)}, bf16[256,512]{1,0:T(8,128)(2,1)S(1)}, u32[]{:S(2)}, u32[]{:S(2)}) collective-permute-start(bf16[256,512]{1,0:T(8,128)(2,1)S(1)} %add_convert_fusion.5), channel_id=1, source_target_pairs={{0,2},{1,3},{2,0},{3,1},{4,6},{5,7},{6,4},{7,5},{8,10},{9,11},{10,... | collective-permute-start | bytes 786440 | tf_op jit(solution)/shard_map/ppermute | solution.py:22
  55.0 11.0 %collective-permute-start.32 = (bf16[256,512]{1,0:T(8,128)(2,1)S(1)}, bf16[256,512]{1,0:T(8,128)(2,1)S(1)}, u32[]{:S(2)}, u32[]{:S(2)}) collective-permute-start(bf16[256,512]{1,0:T(8,128)(2,1)S(1)} %add_convert_fusion.3), channel_id=1, source_target_pairs={{0,2},{1,3},{2,0},{3,1},{4,6},{5,7},{6,4},{7,5},{8,10},{9,11},{10,... | collective-permute-start | bytes 786440 | tf_op jit(solution)/shard_map/ppermute | solution.py:22
  63.3 18.0 %collective-permute-start.12 = (bf16[128,512]{1,0:T(8,128)(2,1)S(1)}, bf16[128,512]{1,0:T(8,128)(2,1)S(1)}, u32[]{:S(2)}, u32[]{:S(2)}) collective-permute-start(bf16[128,512]{1,0:T(8,128)(2,1)S(1)} %get-tuple-element.133), channel_id=1, source_target_pairs={{0,20},{4,16},{8,28},{12,24},{16,4},{20,0},{24,12},{28,8},{1,21},{... | collective-permute-start | bytes 393224 | tf_op jit(solution)/shard_map/ppermute | solution.py:22
  66.0 10.2 %collective-permute-start.21 = (bf16[384,512]{1,0:T(8,128)(2,1)S(1)}, bf16[384,512]{1,0:T(8,128)(2,1)S(1)}, u32[]{:S(2)}, u32[]{:S(2)}) collective-permute-start(bf16[384,512]{1,0:T(8,128)(2,1)S(1)} %add_convert_fusion.1), channel_id=1, source_target_pairs={{0,2},{1,3},{2,0},{3,1},{4,6},{5,7},{6,4},{7,5},{8,10},{9,11},{10,... | collective-permute-start | bytes 1179656 | tf_op jit(solution)/shard_map/ppermute | solution.py:22
  66.6 16.6 %collective-permute-start.11 = (bf16[128,512]{1,0:T(8,128)(2,1)S(1)}, bf16[128,512]{1,0:T(8,128)(2,1)S(1)}, u32[]{:S(2)}, u32[]{:S(2)}) collective-permute-start(bf16[128,512]{1,0:T(8,128)(2,1)S(1)} %get-tuple-element.134), channel_id=1, source_target_pairs={{0,16},{4,20},{8,24},{12,28},{16,0},{20,4},{24,8},{28,12},{1,17},{... | collective-permute-start | bytes 393224 | tf_op jit(solution)/shard_map/ppermute | solution.py:22
  76.2 9.1 %collective-permute-start.34 = (bf16[128,512]{1,0:T(8,128)(2,1)S(1)}, bf16[128,512]{1,0:T(8,128)(2,1)S(1)}, u32[]{:S(2)}, u32[]{:S(2)}) collective-permute-start(bf16[128,512]{1,0:T(8,128)(2,1)S(1)} %get-tuple-element.131), channel_id=1, source_target_pairs={{0,28},{4,24},{8,20},{12,16},{16,12},{20,8},{24,4},{28,0},{1,29},{... | collective-permute-start | bytes 393224 | tf_op jit(solution)/shard_map/ppermute | solution.py:22
  77.3 10.9 %collective-permute-start.33 = (bf16[128,512]{1,0:T(8,128)(2,1)S(1)}, bf16[128,512]{1,0:T(8,128)(2,1)S(1)}, u32[]{:S(2)}, u32[]{:S(2)}) collective-permute-start(bf16[128,512]{1,0:T(8,128)(2,1)S(1)} %get-tuple-element.132), channel_id=1, source_target_pairs={{0,24},{4,28},{8,16},{12,20},{16,8},{20,12},{24,0},{28,4},{1,25},{... | collective-permute-start | bytes 393224 | tf_op jit(solution)/shard_map/ppermute | solution.py:22
  81.3 10.0 %collective-permute-start.23 = (bf16[128,512]{1,0:T(8,128)(2,1)S(1)}, bf16[128,512]{1,0:T(8,128)(2,1)S(1)}, u32[]{:S(2)}, u32[]{:S(2)}) collective-permute-start(bf16[128,512]{1,0:T(8,128)(2,1)S(1)} %get-tuple-element.129), channel_id=1, source_target_pairs={{0,8},{4,12},{8,0},{12,4},{16,24},{20,28},{24,16},{28,20},{1,9},{5... | collective-permute-start | bytes 393224 | tf_op jit(solution)/shard_map/ppermute | solution.py:22
  103.2 10.8 %collective-permute-start.41 = (bf16[512,128]{1,0:T(8,128)(2,1)S(1)}, bf16[512,128]{1,0:T(8,128)(2,1)S(1)}, u32[]{:S(2)}, u32[]{:S(2)}) collective-permute-start(bf16[512,128]{1,0:T(8,128)(2,1)S(1)} %get-tuple-element.123), channel_id=1, source_target_pairs={{0,4},{4,0},{8,12},{12,8},{16,20},{20,16},{24,28},{28,24},{1,5},{5... | collective-permute-start | bytes 393224 | tf_op jit(solution)/shard_map/ppermute | solution.py:22
  108.4 13.3 %collective-permute-start.38 = (bf16[256,128]{1,0:T(8,128)(2,1)S(1)}, bf16[256,128]{1,0:T(8,128)(2,1)S(1)}, u32[]{:S(2)}, u32[]{:S(2)}) collective-permute-start(bf16[256,128]{1,0:T(8,128)(2,1)S(1)} %get-tuple-element.119), channel_id=1, source_target_pairs={{0,4},{4,0},{8,12},{12,8},{16,20},{20,16},{24,28},{28,24},{1,5},{5... | collective-permute-start | bytes 196616 | tf_op jit(solution)/shard_map/ppermute | solution.py:22
  111.1 10.6 %collective-permute-start.39 = (bf16[256,128]{1,0:T(8,128)(2,1)S(1)}, bf16[256,128]{1,0:T(8,128)(2,1)S(1)}, u32[]{:S(2)}, u32[]{:S(2)}) collective-permute-start(bf16[256,128]{1,0:T(8,128)(2,1)S(1)} %get-tuple-element.120), channel_id=1, source_target_pairs={{0,8},{4,12},{8,0},{12,4},{16,24},{20,28},{24,16},{28,20},{1,9},{5... | collective-permute-start | bytes 196616 | tf_op jit(solution)/shard_map/ppermute | solution.py:22
  112.6 9.2 %collective-permute-start.40 = (bf16[256,128]{1,0:T(8,128)(2,1)S(1)}, bf16[256,128]{1,0:T(8,128)(2,1)S(1)}, u32[]{:S(2)}, u32[]{:S(2)}) collective-permute-start(bf16[256,128]{1,0:T(8,128)(2,1)S(1)} %get-tuple-element.121), channel_id=1, source_target_pairs={{0,12},{4,8},{8,4},{12,0},{16,28},{20,24},{24,20},{28,16},{1,13},{... | collective-permute-start | bytes 196616 | tf_op jit(solution)/shard_map/ppermute | solution.py:22
  (28 other events, 318.0 us)
